TPU v7x, 32 devices: a whole 2x2x4 slice. The times are simulated.
32 devices in a mesh: fs: 4 (over z), rep: 4 (over y, x), tp: 2 (over core).
Axes of the slice: x: 2, y: 2, z: 4, core: 2. Of those that a mesh axis runs over, the one named last changes fastest.
Arguments:
- query_input: bfloat16 [16384, 4096], P(('fs', 'rep')), may hold values from -6 to 6
- query_cotangent: bfloat16 [16384, 1024], P(('fs', 'rep'), 'tp'), may hold values from -0.046875 to 0.046875
- branch_output: bfloat16 [16384, 2048], P(('fs', 'rep')), may hold values from -6 to 6
- layer_cotangent: bfloat16 [16384, 4096], P(('fs', 'rep'), 'tp'), may hold values from -0.046875 to 0.046875
- query_weight: float32 [4096, 1024], P(('rep', 'fs'), 'tp'), may hold values from -0.09375 to 0.09375
- output_weight: float32 [2048, 4096], P(('rep', 'fs'), 'tp'), may hold values from -0.125 to 0.125
- query_basis: bfloat16 [4096, 512], P(('rep', 'fs')), may hold values from -0.09375 to 0.09375
- output_basis: bfloat16 [2048, 512], P(('rep', 'fs')), may hold values from -0.125 to 0.125
- query_first: float32 [512, 1024], P(('rep', 'fs'), 'tp'), may hold values from -20 to 20
- query_second: float32 [512, 1024], P(('rep', 'fs'), 'tp'), may hold values from 0.25 to 2
- output_first: float32 [512, 4096], P(('rep', 'fs'), 'tp'), may hold values from -20 to 20
- output_second: float32 [512, 4096], P(('rep', 'fs'), 'tp'), may hold values from 0.25 to 2
Outputs:
- query_update: float32 [4096, 1024], P(('rep', 'fs'), 'tp')
- output_update: float32 [2048, 4096], P(('rep', 'fs'), 'tp')
- query_first_next: float32 [512, 1024], P(('rep', 'fs'), 'tp')
- query_second_next: float32 [512, 1024], P(('rep', 'fs'), 'tp')
- output_first_next: float32 [512, 4096], P(('rep', 'fs'), 'tp')
- output_second_next: float32 [512, 4096], P(('rep', 'fs'), 'tp')
- query_copy: bfloat16 [4096, 1024], P('rep', 'tp')
- output_copy: bfloat16 [2048, 4096], P('rep', 'tp')
All inputs are finite; a program needn't handle non-finite values.
Results may differ from a plain program's by a relative error of at most 0.0055.
Values may be sent and summed in bfloat16 or wider, within the bound.
A program may use at most 128 MiB of HBM per device.

v0:
```python
import functools

import jax
import jax.numpy as jnp
from jax import lax
from jax.experimental import pallas as pl
from jax.experimental.pallas import tpu as pltpu
from jax.sharding import PartitionSpec as P

MESH = pl.DeviceIdType.MESH
DMA = pltpu.SemaphoreType.DMA

beta_first = 0.6
beta_second = 0.8
step_rate = 0.01
small_eps = 1e-06


def here():
    return lax.axis_index("fs"), lax.axis_index("rep"), lax.axis_index("tp")


def flip(rep, bit):
    if bit == 1:
        return rep + 1 - 2 * lax.rem(rep, 2)
    return lax.rem(rep + 2, 4)


def remote(src, dst, send, recv, device):
    return pltpu.make_async_remote_copy(
        src_ref=src, dst_ref=dst, send_sem=send, recv_sem=recv, device_id=device, device_id_type=MESH
    )


def greet(devices):
    barrier = pltpu.get_barrier_semaphore()
    count = 0
    for device, present in devices:
        if present is True:
            pl.semaphore_signal(barrier, inc=1, device_id=device, device_id_type=MESH)
            count = count + 1
        else:
            count = count + present.astype(jnp.int32)

            @pl.when(present)
            def _():
                pl.semaphore_signal(barrier, inc=1, device_id=device, device_id_type=MESH)

    pl.semaphore_wait(barrier, count)


class Line:
    def __init__(self, n, view, send, recv):
        self.n, self.view, self.send_sem, self.recv_sem = n, view, send, recv
        self.fs, self.rep, self.tp = here()
        self.done = 0

    def tick(self):
        if 0 < self.done < self.n:
            self.arrive(self.done)
        if self.done + 1 < self.n:
            self.start(self.done + 1)
        self.done += 1

    def outgoing(self, step, way):
        fs, n = self.fs, self.n
        if way == 0:
            block, peer = fs - step + 1, fs + 1
            present = jnp.logical_and(block >= 0, peer < n)
        else:
            block, peer = fs + step - 1, fs - 1
            present = jnp.logical_and(block < n, peer >= 0)
        block = lax.rem(block + n, n)
        peer = lax.rem(peer + n, n)
        view = self.view(block)
        sems = (self.send_sem.at[way, step - 1], self.recv_sem.at[way, step - 1])
        return remote(view, view, *sems, (peer, self.rep, self.tp)), present

    def incoming(self, step, way):
        fs, n = self.fs, self.n
        block = fs - step if way == 0 else fs + step
        present = block >= 0 if way == 0 else block < n
        block = lax.rem(block + n, n)
        view = self.view(block)
        sems = (self.send_sem.at[way, step - 1], self.recv_sem.at[way, step - 1])
        return remote(view, view, *sems, (fs, self.rep, self.tp)), present, block

    def start(self, step):
        for way in (0, 1):
            copy, present = self.outgoing(step, way)

            @pl.when(present)
            def _():
                copy.start()

    def arrive(self, step):
        for way in (0, 1):
            copy, present, _ = self.incoming(step, way)

            @pl.when(present)
            def _():
                copy.wait_recv()

    def sent(self):
        for step in range(1, self.n):
            for way in (0, 1):
                copy, present = self.outgoing(step, way)

                @pl.when(present)
                def _():
                    copy.wait_send()


def gather(n, views, line_sems, one_sems, two_sems, third_sems=None, ticks=()):
    fs, rep, tp = here()
    lines = [
        Line(n, lambda b, v=v: v(rep * n + b, None), line_sems[0].at[a], line_sems[1].at[a])
        for a, v in enumerate(views)
    ]
    bits = ((1, 2), (2, 1))

    def slots():
        yield 0, 0, 0
        for step in range(1, n):
            yield step, 0, 2 * step - 1
            yield step, 1, 2 * step

    def block_of(step, way):
        if step == 0:
            return fs, True
        block = fs - step if way == 0 else fs + step
        present = block >= 0 if way == 0 else block < n
        return lax.rem(block + n, n), present

    def when(present, body):
        if present is True:
            body()
        else:
            pl.when(present)(body)

    def one(a, block, slot, half):
        peer = flip(rep, bits[half][0])
        view = views[a](rep * n + block, half)
        return remote(view, view, one_sems[0].at[a, half, slot], one_sems[1].at[a, half, slot], (fs, peer, tp))

    def one_in(a, block, slot, half):
        peer = flip(rep, bits[half][0])
        view = views[a](peer * n + block, half)
        return remote(view, view, one_sems[0].at[a, half, slot], one_sems[1].at[a, half, slot], (fs, peer, tp))

    def two(a, block, slot, half, which):
        peer = flip(rep, bits[half][1])
        held = rep if which == 0 else flip(rep, bits[half][0])
        view = views[a](held * n + block, half)
        sems = [s.at[a, half, which, slot] for s in two_sems]
        return remote(view, view, *sems, (fs, peer, tp))

    def two_in(a, block, slot, half, which):
        peer = flip(rep, bits[half][1])
        held = peer if which == 0 else flip(peer, bits[half][0])
        view = views[a](held * n + block, half)
        sems = [s.at[a, half, which, slot] for s in two_sems]
        return remote(view, view, *sems, (fs, peer, tp))

    def third(a, block, group):
        view = views[a](group * n + block, None)
        sems = [s.at[a, group, block] for s in third_sems]
        return remote(view, view, *sems, (fs, rep, 1 - tp))

    def third_in(a, block, group):
        view = views[a](group * n + block, None, 1 - tp)
        sems = [s.at[a, group, block] for s in third_sems]
        return remote(view, view, *sems, (fs, rep, 1 - tp))

    arrays = range(len(views))

    def launch(step, way, slot):
        block, present = block_of(step, way)

        def body():
            for a in arrays:
                for half in (0, 1):
                    one(a, block, slot, half).start()
                for half in (0, 1):
                    two(a, block, slot, half, 0).start()

        when(present, body)

    def relay(step, way, slot):
        block, present = block_of(step, way)

        def body():
            for a in arrays:
                for half in (0, 1):
                    one_in(a, block, slot, half).wait_recv()
                    two(a, block, slot, half, 1).start()

        when(present, body)

    def finish(step, way, slot):
        block, present = block_of(step, way)

        def body():
            for a in arrays:
                for half in (0, 1):
                    for which in (0, 1):
                        two_in(a, block, slot, half, which).wait_recv()
                if third_sems is not None:
                    for group in range(4):
                        third(a, block, group).start()

        when(present, body)

    def drain(step, way, slot):
        block, present = block_of(step, way)

        def body():
            for a in arrays:
                for half in (0, 1):
                    one(a, block, slot, half).wait_send()
                    for which in (0, 1):
                        two(a, block, slot, half, which).wait_send()
                if third_sems is not None:
                    for group in range(4):
                        third(a, block, group).wait_send()
                        third_in(a, block, group).wait_recv()

        when(present, body)

    order = list(slots())
    for step in range(n):
        if step:
            for line in lines:
                line.arrive(step)
        if step < n - 1:
            for line in lines:
                line.start(step + 1)
        if step == n - 2:
            for side in ticks:
                side.tick()
        for s, way, slot in order:
            if s == step:
                launch(s, way, slot)
        for s, way, slot in order:
            if s == step - 1:
                relay(s, way, slot)
            if s == step - 2:
                finish(s, way, slot)
    for side in ticks:
        side.tick()
    for s, way, slot in order:
        if s == n - 1:
            relay(s, way, slot)
        if s == n - 2:
            finish(s, way, slot)
    for side in ticks:
        side.tick()
    for s, way, slot in order:
        if s == n - 1:
            finish(s, way, slot)
    for side in ticks:
        while side.done < n:
            side.tick()
    for s, way, slot in order:
        drain(s, way, slot)
    for line in lines:
        line.sent()


def pairs(*shapes):
    return [DMA(shape) for shape in shapes for _ in (0, 1)]


def first_kernel(
    n, bq_ref, bo_ref, w_ref, v_ref, gq_ref, go_ref, gw_ref, gv_ref,
    local, ls, lr, os, orr, ts, tr, hs, hr, ws, wr,
):
    fs, rep, tp = here()
    mine = rep * n + fs
    copies = [
        pltpu.make_async_copy(bq_ref, gq_ref.at[mine], local.at[0]),
        pltpu.make_async_copy(bo_ref, go_ref.at[mine], local.at[1]),
        pltpu.make_async_copy(w_ref, gw_ref.at[fs], local.at[2]),
        pltpu.make_async_copy(v_ref, gv_ref.at[fs], local.at[3]),
    ]
    for copy in copies:
        copy.start()
    peers = [((lax.rem(fs + 1, n), rep, tp), fs + 1 < n), ((lax.rem(fs + n - 1, n), rep, tp), fs >= 1)]
    peers += [((fs, flip(rep, bit), tp), True) for bit in (1, 2)]
    peers += [((fs, rep, 1 - tp), True)]
    for copy in copies:
        copy.wait()
    greet(peers)

    def view_of(ref):
        rows, cols = ref.shape[1] // 2, ref.shape[2] // 2

        def view(block, half, core=None):
            core = tp if core is None else core
            span = pl.ds(pl.multiple_of(core * cols, cols), cols)
            if half is None:
                return ref.at[block, :, span]
            return ref.at[block, pl.ds(half * rows, rows), span]

        return view

    weights = [
        Line(n, lambda b, g=g: g.at[b], ws.at[i], wr.at[i]) for i, g in enumerate((gw_ref, gv_ref))
    ]
    gather(
        n, [view_of(gq_ref), view_of(go_ref)], (ls, lr), (os, orr), (ts, tr), (hs, hr), ticks=weights
    )
    for side in weights:
        side.sent()


def gather_bases(n, basis_q, basis_o, *weights):
    slots = 2 * n - 1
    whole = lambda a: jax.ShapeDtypeStruct((4 * n, *a.shape), a.dtype)
    vmem = pl.BlockSpec(memory_space=pltpu.VMEM)
    return pl.pallas_call(
        functools.partial(first_kernel, n),
        out_shape=(whole(basis_q), whole(basis_o))
        + tuple(jax.ShapeDtypeStruct((n, *w.shape), w.dtype) for w in weights),
        in_specs=[vmem] * 4,
        out_specs=(vmem,) * 4,
        scratch_shapes=[DMA((4,))]
        + pairs((2, 2, n - 1), (2, 2, slots), (2, 2, 2, slots), (2, 4, n), (2, 2, n - 1)),
        compiler_params=pltpu.CompilerParams(
            collective_id=0, has_side_effects=True, vmem_limit_bytes=40 * 2**20
        ),
        name="gather_bases",
    )(basis_q, basis_o, *weights)


def second_kernel(
    n, pq_ref, po_ref, fq_ref, sq_ref, fo_ref, so_ref, w_ref,
    nfq_ref, nsq_ref, nfo_ref, nso_ref, gq_ref, go_ref, gw_ref, tot_ref,
    rq, ro, aq, ao, zq, zo, gs, local,
    rs, rr, zs, zr, ls, lr, os, orr, ts, tr, ws, wr, cs, cr,
):
    fs, rep, tp = here()
    mine = rep * n + fs
    own = pltpu.make_async_copy(w_ref, gw_ref.at[fs], local.at[0])
    own.start()
    peers = [((lax.rem(fs + k, n), rep, tp), True) for k in range(1, n)]
    peers += [((fs, lax.rem(rep + k, 4), tp), True) for k in range(1, 4)]
    peers += [((fs, rep, 1 - tp), True)]
    own.wait()
    greet(peers)
    weights = Line(n, lambda b: gw_ref.at[b], ws, wr)

    parts, heard, summed, late = (pq_ref, po_ref), (rq, ro), (aq, ao), (zq, zo)

    def swap(a, j, k):
        f, to = lax.rem(fs + j, n), lax.rem(rep + k, 4)
        sems = (rs.at[a, j - 1, k - 1], rr.at[a, j - 1, k - 1])
        return remote(parts[a].at[to * n + f], heard[a].at[j - 1, k - 1], *sems, (fs, to, tp))

    def cross(a, j):
        f = lax.rem(fs + j, n)
        return remote(
            summed[a].at[j - 1], late[a].at[j - 1], zs.at[a, j - 1], zr.at[a, j - 1], (f, rep, tp)
        )

    for j in range(1, n + 1):
        for a in (1, 0):
            for k in (2, 1, 3):
                swap(a, j, k).start()
    weights.tick()
    final = [None, None]
    for j in range(1, n + 1):
        f = lax.rem(fs + j, n)
        for a in (1, 0):
            for k in (2, 1, 3):
                swap(a, j, k).wait_recv()
            total = parts[a][rep * n + f].astype(jnp.float32)
            for k in (1, 2, 3):
                total = total + heard[a][j - 1, k - 1].astype(jnp.float32)
            if j < n:
                summed[a][j - 1] = total.astype(jnp.bfloat16)
                cross(a, j).start()
            else:
                final[a] = total
    for a in (0, 1):
        for j in range(1, n):
            cross(a, j).wait_recv()
        for j in range(1, n):
            final[a] = final[a] + late[a][j - 1].astype(jnp.float32)
    refs = ((fq_ref, sq_ref, nfq_ref, nsq_ref, gq_ref), (fo_ref, so_ref, nfo_ref, nso_ref, go_ref))
    for a in (0, 1):
        first, second, first_out, second_out, g = refs[a]
        first_next = beta_first * first[...] + (1.0 - beta_first) * final[a]
        second_next = beta_second * second[...] + (1.0 - beta_second) * final[a] * final[a]
        normed = first_next / jnp.sqrt(second_next)
        first_out[...] = first_next
        second_out[...] = second_next
        g[mine] = normed.astype(jnp.bfloat16)
        square = normed * normed
        rows, cols = square.shape
        square = sum(square[:, c : c + 128] for c in range(0, cols, 128))
        square = sum(square[r : r + 8] for r in range(0, rows, 8))
        gs[mine, :, a * 128 : (a + 1) * 128] = square

    def view_of(ref):
        cols = ref.shape[2] // 2

        def view(block, half):
            if half is None:
                return ref.at[block]
            return ref.at[block, :, pl.ds(half * cols, cols)]

        return view

    gather(n, [view_of(go_ref), view_of(gq_ref), view_of(gs)], (ls, lr), (os, orr), (ts, tr), ticks=[weights])
    tot_ref[0] = sum(gs[b] for b in range(4 * n))
    pair = remote(tot_ref.at[0], tot_ref.at[1], cs.at[0], cr.at[0], (fs, rep, 1 - tp))
    pair.start()
    pair.wait()
    weights.sent()
    for j in range(1, n + 1):
        for a in (0, 1):
            for k in (1, 2, 3):
                swap(a, j, k).wait_send()
            if j < n:
                cross(a, j).wait_send()


def advance(n, part_q, part_o, first_q, second_q, first_o, second_o, weight):
    slots = 2 * n - 1
    rows, cq = first_q.shape
    co = first_o.shape[1]
    f32, b16 = jnp.float32, jnp.bfloat16
    shape = jax.ShapeDtypeStruct
    vmem = pl.BlockSpec(memory_space=pltpu.VMEM)
    return pl.pallas_call(
        functools.partial(second_kernel, n),
        out_shape=(
            shape((rows, cq), f32), shape((rows, cq), f32), shape((rows, co), f32), shape((rows, co), f32),
            shape((4 * n, rows, cq), b16), shape((4 * n, rows, co), b16),
            shape((n, *weight.shape), b16), shape((2, 8, 256), f32),
        ),
        in_specs=[vmem] * 7,
        out_specs=(vmem,) * 8,
        scratch_shapes=[
            pltpu.VMEM((n, 3, rows, cq), b16), pltpu.VMEM((n, 3, rows, co), b16),
            pltpu.VMEM((n - 1, rows, cq), b16), pltpu.VMEM((n - 1, rows, co), b16),
            pltpu.VMEM((n - 1, rows, cq), b16), pltpu.VMEM((n - 1, rows, co), b16),
            pltpu.VMEM((4 * n, 8, 256), f32), DMA((1,)),
        ]
        + pairs((2, n, 3), (2, n - 1), (3, 2, n - 1), (3, 2, slots), (3, 2, 2, slots), (2, n - 1), (1,)),
        compiler_params=pltpu.CompilerParams(
            collective_id=1, has_side_effects=True, vmem_limit_bytes=48 * 2**20
        ),
        name="advance",
    )(part_q, part_o, first_q, second_q, first_o, second_o, weight)


def body(
    n,
    query_input,
    query_cotangent,
    branch_output,
    layer_cotangent,
    query_weight,
    output_weight,
    query_basis,
    output_basis,
    query_first,
    query_second,
    output_first,
    output_second,
):
    f32, b16 = jnp.float32, jnp.bfloat16
    rank = query_basis.shape[1]
    half = output_weight.shape[0] // 2
    near, far = output_weight[:half].astype(b16), output_weight[half:].astype(b16)
    gq, go, wq, wo_near = gather_bases(n, query_basis, output_basis, query_weight.astype(b16), near)
    whole_q, whole_o = gq.reshape(-1, rank), go.reshape(-1, rank)

    def project(inputs, basis, cotangent):
        inner = jnp.dot(inputs, basis, preferred_element_type=f32).astype(b16)
        part = lax.dot_general(inner, cotangent, (((0,), (0,)), ((), ())), preferred_element_type=f32)
        return part.astype(b16).reshape(4 * n, -1, cotangent.shape[1])

    part_q = project(query_input, whole_q, query_cotangent)
    part_o = project(branch_output, whole_o, layer_cotangent)
    first_q, second_q, first_o, second_o, nq, no, wo_far, totals = advance(
        n, part_q, part_o, query_first, query_second, output_first, output_second, far
    )
    sums = jnp.sum(totals.reshape(16, 2, 128), axis=(0, 2))
    rep = lax.axis_index("rep")

    def update(basis, whole, normed, total, weights):
        normed = normed.reshape(rank, -1)
        columns = normed.shape[1]
        scale = lax.rsqrt(total / (rank * 2 * columns) + small_eps)
        mine = scale * jnp.dot(basis, normed, preferred_element_type=f32)
        weights = weights.reshape(-1, columns)
        count = weights.shape[0]
        rows = lax.dynamic_slice_in_dim(whole, rep * count, count)
        group = scale * jnp.dot(rows, normed, preferred_element_type=f32)
        return mine, (weights.astype(f32) - step_rate * group).astype(b16)

    update_q, copy_q = update(query_basis, whole_q, nq, sums[0], wq)
    update_o, copy_o = update(output_basis, whole_o, no, sums[1], jnp.concatenate([wo_near, wo_far], axis=1))
    return (update_q, update_o, first_q, second_q, first_o, second_o, copy_q, copy_o)


def solution(mesh):
    in_specs = (
        P(("fs", "rep"), None),
        P(("fs", "rep"), "tp"),
        P(("fs", "rep"), None),
        P(("fs", "rep"), "tp"),
        P(("rep", "fs"), "tp"),
        P(("rep", "fs"), "tp"),
        P(("rep", "fs"), None),
        P(("rep", "fs"), None),
        P(("rep", "fs"), "tp"),
        P(("rep", "fs"), "tp"),
        P(("rep", "fs"), "tp"),
        P(("rep", "fs"), "tp"),
    )
    out_specs = (
        P(("rep", "fs"), "tp"),
        P(("rep", "fs"), "tp"),
        P(("rep", "fs"), "tp"),
        P(("rep", "fs"), "tp"),
        P(("rep", "fs"), "tp"),
        P(("rep", "fs"), "tp"),
        P("rep", "tp"),
        P("rep", "tp"),
    )
    n = mesh.shape["fs"]
    assert mesh.shape["rep"] == 4 and mesh.shape["tp"] == 2
    return jax.shard_map(functools.partial(body, n), mesh=mesh, in_specs=in_specs, out_specs=out_specs, check_vma=False)
```

profile of v0, /device:TPU:0, one launch (start us, length us, event | category | flops | bytes accessed | tf_op | source)
XLA Modules:
  0.0 176.4 jit_solution(659522946599924232)
XLA Ops:
  0.6 1.4 convert.6
  2.1 1.1 convert_element_type.37.w_ref
  3.2 0.9 copy-done.1
  4.1 0.9 copy-done.7
  5.0 56.6 %gather_bases.1 = (bf16[16,256,512]{2,1,0:T(8,128)(2,1)S(1)}, bf16[16,128,512]{2,1,0:T(8,128)(2,1)S(1)}, bf16[4,256,512]{2,1,0:T(8,128)(2,1)S(1)}, bf16[4,64,2048]{2,1,0:T(8,128)(2,1)S(1)}) custom-call(bf16[256,512]{1,0:T(8,128)(2,1)S(1)} %copy-done.1, bf16[128,512]{1,0:T(8,128)(2,1)S(1)} %copy-done.7, bf16[256,512]{1,0:T(8,128)(2,1)S(1)} %convert_element_type.37.w_ref, ...), custom_call_target="tpu_custom_call" | custom-call | tf_op jit(solution)/shard_map/gather_bases/pallas_call | solution.py:321
  61.6 1.9 %copy-done.21 = bf16[16,256,512]{2,1,0:T(8,128)(2,1)} copy-done((bf16[16,256,512]{2,1,0:T(8,128)(2,1)}, bf16[16,256,512]{2,1,0:T(8,128)(2,1)S(1)}, u32[]{:S(2)}) %copy-start.21) | copy-done | bytes 4194328
  63.6 1.3 copy-done.22
  64.9 1.0 copy-done.23
  65.9 10.3 %convolution_convert_fusion = bf16[512,2048]{1,0:T(8,128)(2,1)} fusion(bf16[1024,2048]{1,0:T(8,128)(2,1)} %param.15, bf16[2048,512]{1,0:T(8,128)(2,1)} %bitcast.37, bf16[1024,2048]{1,0:T(8,128)(2,1)} %param.14), kind=kOutput, calls=%fused_computation.2 | convolution fusion | flops 4296540160 | bytes 12582912 | tf_op jit(solution)/shard_map/dot_general | solution.py:483
  76.2 10.6 %convolution_convert_fusion.3 = bf16[512,512]{1,0:T(8,128)(2,1)} fusion(bf16[1024,512]{1,0:T(8,128)(2,1)S(1)} %copy-done, bf16[4096,512]{1,0:T(8,128)(2,1)} %bitcast.35, bf16[1024,4096]{1,0:T(8,128)(2,1)} %param.12), kind=kOutput, calls=%fused_computation.10 | convolution fusion | flops 4832624640 | bytes 14155776 | tf_op jit(solution)/shard_map/dot_general | solution.py:483
  86.8 1.1 copy-done.6
  87.9 0.9 copy-done.9
  88.9 0.9 copy-done.10
  89.8 65.4 %advance.1 = (f32[32,512]{1,0:T(8,128)S(1)}, f32[32,512]{1,0:T(8,128)S(1)}, f32[32,2048]{1,0:T(8,128)S(1)}, f32[32,2048]{1,0:T(8,128)S(1)}, bf16[16,32,512]{2,1,...) custom-call(bf16[16,32,512]{2,1,0:T(8,128)(2,1)S(1)} %bitcast.34, ...), custom_call_target="tpu_custom_call" | custom-call | tf_op jit(solution)/shard_map/advance/pallas_call | solution.py:436
  155.3 1.6 pad_maximum_fusion
  158.4 4.4 %fusion = bf16[512,2048]{1,0:T(8,128)(2,1)} fusion(bf16[512,2048]{1,0:T(8,128)(2,1)} %bitcast.41, bf16[512,2048]{1,0:T(8,128)(2,1)S(1)} %bitcast.30, f32[]{:T(128)} %bitcast.8, bf16[2048,512]{1,0:T(8,128)(2,1)} %bitcast.38, s32[]{:T(128)S(6)} %select_n.7), kind=kOutput, calls=%fused_computation.1 | convolution fusion | flops 1078984704 | bytes 6816260 | tf_op jit(solution)/shard_map/dot_general | solution.py:502
  163.6 3.4 %fusion.2 = bf16[1024,512]{1,0:T(8,128)(2,1)} fusion(bf16[1024,512]{1,0:T(8,128)(2,1)} %bitcast.39, bf16[512,512]{1,0:T(8,128)(2,1)} %bitcast.32, bf16[4096,512]{1,0:T(8,128)(2,1)} %bitcast.36, s32[]{:T(128)S(6)} %select_n.6, f32[]{:T(128)} %bitcast.5), kind=kOutput, calls=%fused_computation.7 | convolution fusion | flops 539492352 | bytes 3670532 | tf_op jit(solution)/shard_map/dot_general | solution.py:502
  167.0 1.7 fusion.1
  168.8 2.6 %copy.23 = f32[128,2048]{1,0:T(8,128)} copy(f32[128,2048]{0,1:T(8,128)} %fusion.1) | data formatting | bytes 2097152
  171.4 1.4 fusion.3
  172.7 1.0 copy.22
  173.7 0.6 copy.28
  175.0 0.7 copy.30
  175.7 0.7 copy.31
  (45 shorter events, 1.5 us)
Async XLA Ops:
  0.6 75.6 %copy-start = (bf16[1024,512]{1,0:T(8,128)(2,1)S(1)}, bf16[1024,512]{1,0:T(8,128)(2,1)}, u32[]{:S(2)}) copy-start(bf16[1024,512]{1,0:T(8,128)(2,1)} %param.13) | copy-start | bytes 3145732
  3.2 1.0 copy-start.1
  4.1 0.9 copy-start.7
  61.6 1.9 %copy-start.21 = (bf16[16,256,512]{2,1,0:T(8,128)(2,1)}, bf16[16,256,512]{2,1,0:T(8,128)(2,1)S(1)}, u32[]{:S(2)}) copy-start(bf16[16,256,512]{2,1,0:T(8,128)(2,1)S(1)} %get-tuple-element.20) | copy-start | bytes 12582916
  63.6 1.3 copy-start.22
  64.9 1.0 copy-start.23
  65.9 10.3 %copy-start.3 = (bf16[4,64,2048]{2,1,0:T(8,128)(2,1)}, bf16[4,64,2048]{2,1,0:T(8,128)(2,1)S(1)}, u32[]{:S(2)}) copy-start(bf16[4,64,2048]{2,1,0:T(8,128)(2,1)S(1)} %get-tuple-element.30) | copy-start | bytes 3145732
  76.2 10.6 %copy-start.15 = (f32[32,512]{1,0:T(8,128)S(1)}, f32[32,512]{1,0:T(8,128)}, u32[]{:S(2)}) copy-start(f32[32,512]{1,0:T(8,128)} %fq_ref.1) | copy-start | bytes 196612
  76.2 10.6 %copy-start.16 = (f32[32,512]{1,0:T(8,128)S(1)}, f32[32,512]{1,0:T(8,128)}, u32[]{:S(2)}) copy-start(f32[32,512]{1,0:T(8,128)} %sq_ref.1) | copy-start | bytes 196612
  86.8 68.5 %copy-start.4 = (bf16[4,64,2048]{2,1,0:T(8,128)(2,1)S(1)}, bf16[4,64,2048]{2,1,0:T(8,128)(2,1)}, u32[]{:S(2)}) copy-start(bf16[4,64,2048]{2,1,0:T(8,128)(2,1)} %copy-done.3) | copy-start | bytes 3145732
  86.8 1.1 copy-start.6
  87.9 0.9 copy-start.9
  88.9 0.9 copy-start.10
  155.2 1.7 copy-start.5
  155.2 1.7 copy-start.11
  155.3 1.7 copy-start.13
  155.3 1.7 copy-start.17
  155.3 1.7 copy-start.19
  162.8 4.2 %copy-start.8 = (bf16[128,512]{1,0:T(8,128)(2,1)S(1)}, bf16[128,512]{1,0:T(8,128)(2,1)}, u32[]{:S(2)}) copy-start(bf16[128,512]{1,0:T(8,128)(2,1)} %bo_ref.1) | copy-start | bytes 393220
  167.0 4.4 %copy-start.2 = (bf16[256,512]{1,0:T(8,128)(2,1)S(1)}, bf16[256,512]{1,0:T(8,128)(2,1)}, u32[]{:S(2)}) copy-start(bf16[256,512]{1,0:T(8,128)(2,1)} %bq_ref.1) | copy-start | bytes 786436
  168.7 5.0 %copy-start.20 = (f32[32,512]{1,0:T(8,128)S(1)}, f32[32,512]{1,0:T(8,128)}, u32[]{:S(2)}) copy-start(f32[32,512]{1,0:T(8,128)} %copy-done.19) | copy-start | bytes 196612
  168.8 5.6 %copy-start.18 = (f32[32,512]{1,0:T(8,128)S(1)}, f32[32,512]{1,0:T(8,128)}, u32[]{:S(2)}) copy-start(f32[32,512]{1,0:T(8,128)} %copy-done.17) | copy-start | bytes 196612
  168.8 6.3 %copy-start.14 = (f32[32,2048]{1,0:T(8,128)S(1)}, f32[32,2048]{1,0:T(8,128)}, u32[]{:S(2)}) copy-start(f32[32,2048]{1,0:T(8,128)} %copy-done.13) | copy-start | bytes 786436
  168.8 7.0 %copy-start.12 = (f32[32,2048]{1,0:T(8,128)S(1)}, f32[32,2048]{1,0:T(8,128)}, u32[]{:S(2)}) copy-start(f32[32,2048]{1,0:T(8,128)} %copy-done.11) | copy-start | bytes 786436
where the time goes:
time: 177 us; the launch traced here: 176 us
  Pallas kernels  122 us (69%)
  matrix products  31.9 us (18%)
  local copies, waits for them, and re-layouts  16.1 us (9%)
  other arithmetic  4.22 us (2%)
  between operations  2.24 us (1%)
    pallas_call x1, Pallas kernels, advance(): pl.pallas_call(functools.partial(second_kernel, n), out_shape=(shape((row...  65.4 us
    pallas_call x1, Pallas kernels, gather_bases(): pl.pallas_call(functools.partial(first_kernel, n), out_shape=(whole(basis...  56.6 us
    dot_general x2, matrix products, project(): lax.dot_general(inner, cotangent, (((0,), (0,)), ((), ())), preferred_ele...  20.9 us
    unnamed x54, local copies, waits for them, and re-layouts  15.5 us
    dot_general x2, matrix products, update(): group = scale * jnp.dot(rows, normed, preferred_element_type=f32)  7.88 us

commit v1 on v0

v1 whole, which is shorter than its diff:
```python
import functools

import jax
import jax.numpy as jnp
from jax import lax
from jax.experimental import pallas as pl
from jax.experimental.pallas import tpu as pltpu
from jax.sharding import PartitionSpec as P

MESH = pl.DeviceIdType.MESH
DMA = pltpu.SemaphoreType.DMA

beta_first = 0.6
beta_second = 0.8
step_rate = 0.01
small_eps = 1e-06


def here():
    return lax.axis_index("fs"), lax.axis_index("rep"), lax.axis_index("tp")


def flip(rep, bit):
    if bit == 1:
        return rep + 1 - 2 * lax.rem(rep, 2)
    return lax.rem(rep + 2, 4)


def remote(src, dst, send, recv, device):
    return pltpu.make_async_remote_copy(
        src_ref=src, dst_ref=dst, send_sem=send, recv_sem=recv, device_id=device, device_id_type=MESH
    )


def greet(devices):
    barrier = pltpu.get_barrier_semaphore()
    for device in devices:
        pl.semaphore_signal(barrier, inc=1, device_id=device, device_id_type=MESH)
    pl.semaphore_wait(barrier, len(devices))


class Line:
    def __init__(self, n, view, send, recv):
        self.n, self.view, self.send_sem, self.recv_sem = n, view, send, recv
        self.fs, self.rep, self.tp = here()
        self.done = 0

    def tick(self):
        if 0 < self.done < self.n:
            self.arrive(self.done)
        if self.done + 1 < self.n:
            self.start(self.done + 1)
        self.done += 1

    def outgoing(self, step, way):
        fs, n = self.fs, self.n
        if way == 0:
            block, peer = fs - step + 1, fs + 1
            present = jnp.logical_and(block >= 0, peer < n)
        else:
            block, peer = fs + step - 1, fs - 1
            present = jnp.logical_and(block < n, peer >= 0)
        block = lax.rem(block + n, n)
        peer = lax.rem(peer + n, n)
        view = self.view(block)
        sems = (self.send_sem.at[way, step - 1], self.recv_sem.at[way, step - 1])
        return remote(view, view, *sems, (peer, self.rep, self.tp)), present

    def incoming(self, step, way):
        fs, n = self.fs, self.n
        block = fs - step if way == 0 else fs + step
        present = block >= 0 if way == 0 else block < n
        block = lax.rem(block + n, n)
        view = self.view(block)
        sems = (self.send_sem.at[way, step - 1], self.recv_sem.at[way, step - 1])
        return remote(view, view, *sems, (fs, self.rep, self.tp)), present, block

    def start(self, step):
        for way in (0, 1):
            copy, present = self.outgoing(step, way)

            @pl.when(present)
            def _():
                copy.start()

    def arrive(self, step):
        for way in (0, 1):
            copy, present, _ = self.incoming(step, way)

            @pl.when(present)
            def _():
                copy.wait_recv()

    def sent(self):
        for step in range(1, self.n):
            for way in (0, 1):
                copy, present = self.outgoing(step, way)

                @pl.when(present)
                def _():
                    copy.wait_send()


def when(present, body):
    if present is True:
        body()
    else:
        pl.when(present)(body)


class Gather:
    bits = ((1, 2), (2, 1))

    def __init__(self, n, view, line_sems, one_sems, two_sems):
        self.n, self.view, self.one_sems, self.two_sems = n, view, one_sems, two_sems
        self.fs, self.rep, self.tp = here()
        self.line = Line(n, lambda b: view(self.rep * n + b, None), *line_sems)

    def slots(self, step):
        return [(0, 0)] if step == 0 else [(0, 2 * step - 1), (1, 2 * step)]

    def block_of(self, step, way):
        if step == 0:
            return self.fs, True
        block = self.fs - step if way == 0 else self.fs + step
        present = block >= 0 if way == 0 else block < self.n
        return lax.rem(block + self.n, self.n), present

    def one(self, block, slot, half):
        peer = flip(self.rep, self.bits[half][0])
        view = self.view(self.rep * self.n + block, half)
        return remote(view, view, *[s.at[half, slot] for s in self.one_sems], (self.fs, peer, self.tp))

    def one_in(self, block, slot, half):
        peer = flip(self.rep, self.bits[half][0])
        view = self.view(peer * self.n + block, half)
        return remote(view, view, *[s.at[half, slot] for s in self.one_sems], (self.fs, peer, self.tp))

    def two(self, block, slot, half, which):
        peer = flip(self.rep, self.bits[half][1])
        held = self.rep if which == 0 else flip(self.rep, self.bits[half][0])
        view = self.view(held * self.n + block, half)
        return remote(view, view, *[s.at[half, which, slot] for s in self.two_sems], (self.fs, peer, self.tp))

    def two_in(self, block, slot, half, which):
        peer = flip(self.rep, self.bits[half][1])
        held = peer if which == 0 else flip(peer, self.bits[half][0])
        view = self.view(held * self.n + block, half)
        return remote(view, view, *[s.at[half, which, slot] for s in self.two_sems], (self.fs, peer, self.tp))

    def each(self, step, action):
        for way, slot in self.slots(step):
            block, present = self.block_of(step, way)
            when(present, lambda: action(block, slot))

    def launch(self, step):
        def action(block, slot):
            for half in (0, 1):
                self.one(block, slot, half).start()
            for half in (0, 1):
                self.two(block, slot, half, 0).start()

        self.each(step, action)

    def start(self):
        self.line.start(1)
        self.launch(0)

    def arrive(self, step):
        self.line.arrive(step)
        if step < self.n - 1:
            self.line.start(step + 1)
        self.launch(step)

    def relay(self, step):
        def action(block, slot):
            for half in (0, 1):
                self.one_in(block, slot, half).wait_recv()
                self.two(block, slot, half, 1).start()

        self.each(step, action)

    def finish(self, step):
        def action(block, slot):
            for half in (0, 1):
                for which in (0, 1):
                    self.two_in(block, slot, half, which).wait_recv()

        self.each(step, action)

    def drain(self):
        def action(block, slot):
            for half in (0, 1):
                self.one(block, slot, half).wait_send()
                for which in (0, 1):
                    self.two(block, slot, half, which).wait_send()

        for step in range(self.n):
            self.each(step, action)
        self.line.sent()


class Scatter:
    def __init__(self, n, part, one, mid, two, total, out, late, one_sems, two_sems, line_sems):
        self.n, self.part, self.heard, self.mid_ref, self.two = n, part, one, mid, two
        self.total, self.out, self.late = total, out, late
        self.one_sems, self.two_sems, self.line_sems = one_sems, two_sems, line_sems
        self.fs, self.rep, self.tp = here()
        self.chunks, _, group, self.width = part.shape
        self.rows = group // n

    def peers(self, c):
        first, second = ((1, 2), (2, 1))[c % 2]
        return flip(self.rep, first), flip(self.rep, second), second

    def first(self, c, slot):
        near, _, second = self.peers(c)
        group = near if slot == 0 else flip(near, second)
        sems = [s.at[c, slot] for s in self.one_sems]
        return remote(self.part.at[c, group], self.heard.at[c, slot], *sems, (self.fs, near, self.tp))

    def second(self, c):
        _, far, _ = self.peers(c)
        sems = [s.at[c] for s in self.two_sems]
        return remote(self.mid_ref.at[c], self.two.at[c], *sems, (self.fs, far, self.tp))

    def third(self, c, j):
        f = lax.rem(self.fs + j, self.n)
        sems = [s.at[c, j - 1] for s in self.line_sems]
        return remote(self.out.at[c, j - 1], self.late.at[c, j - 1], *sems, (f, self.rep, self.tp))

    def compute(self, c, inner, cotangent):
        tile = min(256, self.width)
        rank = inner.shape[0] * inner.shape[1]

        def step(i, _):
            span = pl.ds(pl.multiple_of(c * self.width + i * tile, tile), tile)
            value = jnp.dot(
                inner[...].reshape(rank, -1), cotangent[:, span], preferred_element_type=jnp.float32
            )
            here_span = pl.ds(pl.multiple_of(i * tile, tile), tile)
            self.part[c, :, :, here_span] = value.astype(jnp.bfloat16).reshape(4, -1, tile)
            return 0

        lax.fori_loop(0, self.width // tile, step, 0)

    def send(self, c):
        for slot in (1, 0):
            self.first(c, slot).start()

    def middle(self, c):
        f32 = jnp.float32
        _, far, _ = self.peers(c)
        self.first(c, 1).wait_recv()
        value = self.part[c, far].astype(f32) + self.heard[c, 1].astype(f32)
        self.mid_ref[c] = value.astype(jnp.bfloat16)
        self.second(c).start()
        self.first(c, 0).wait_recv()
        self.total[c] = self.part[c, self.rep].astype(f32) + self.heard[c, 0].astype(f32)

    def rows_of(self, c, f):
        span = pl.ds(pl.multiple_of(f * self.rows, self.rows), self.rows)
        return self.total[c, span, :] + self.two[c, span, :].astype(jnp.float32)

    def cross(self, c):
        self.second(c).wait_recv()
        for j in range(1, self.n):
            value = self.rows_of(c, lax.rem(self.fs + j, self.n))
            self.out[c, j - 1] = value.astype(jnp.bfloat16)
            self.third(c, j).start()

    def final(self, c):
        value = self.rows_of(c, self.fs)
        for j in range(1, self.n):
            self.third(c, j).wait_recv()
            value = value + self.late[c, j - 1].astype(jnp.float32)
        return value

    def drain(self):
        for c in range(self.chunks):
            for slot in (0, 1):
                self.first(c, slot).wait_send()
            self.second(c).wait_send()
            for j in range(1, self.n):
                self.third(c, j).wait_send()


class Weights:
    def __init__(self, n, views, send, recv):
        self.lines = [Line(n, v, send.at[i], recv.at[i]) for i, v in enumerate(views)]
        self.n = n
        self.todo = [(step, line) for step in range(1, n) for line in self.lines]

    def tick(self, count):
        for _ in range(count):
            if self.todo:
                step, line = self.todo.pop(0)
                if step > 1:
                    line.arrive(step - 1)
                line.start(step)

    def finish(self):
        self.tick(len(self.todo))
        for line in self.lines:
            line.arrive(self.n - 1)

    def sent(self):
        for line in self.lines:
            line.sent()


def main_kernel(
    n,
    xq_hbm, cq_hbm, xo_hbm, co_hbm, wq_hbm, wo_hbm, bq_hbm, bo_hbm, fq_hbm, sq_hbm, fo_hbm, so_hbm,
    nq_ref, no_ref, gwq_ref, gwo_ref, hq_ref, ho_ref, nfq_ref, nsq_ref, nfo_ref, nso_ref, tot_ref,
    xq, cq, xo, co, wq, wo, fq, sq, fo, so, gbq, gbo, inq, ino,
    part_q, one_q, mid_q, two_q, total_q, out_q, late_q,
    part_o, one_o, mid_o, two_o, total_o, out_o, late_o,
    gs, local, *sems,
):
    fs, rep, tp = here()
    mine = rep * n + fs
    f32, b16 = jnp.float32, jnp.bfloat16
    sems = list(sems)

    def take():
        pair = (sems.pop(0), sems.pop(0))
        return pair

    half = bq_hbm.shape[1] // 2
    own = pl.ds(pl.multiple_of(tp * half, half), half)
    copies = [
        pltpu.make_async_copy(src, dst, local.at[i])
        for i, (src, dst) in enumerate(
            [
                (bo_hbm.at[:, own], gbo.at[mine]), (bq_hbm.at[:, own], gbq.at[mine]),
                (wq_hbm, wq), (wo_hbm, wo), (xo_hbm, xo), (co_hbm, co), (xq_hbm, xq), (cq_hbm, cq),
                (fo_hbm, fo), (so_hbm, so), (fq_hbm, fq), (sq_hbm, sq),
            ]
        )
    ]
    for copy in copies:
        copy.start()
    copies[0].wait()
    copies[1].wait()
    peers = [(lax.rem(fs + k, n), rep, tp) for k in range(1, n)]
    peers += [(fs, flip(rep, bit), tp) for bit in (1, 2)] + [(fs, rep, 1 - tp)]
    greet(peers)

    def rows_view(ref):
        rows = ref.shape[1] // 2

        def view(block, part):
            return ref.at[block] if part is None else ref.at[block, pl.ds(part * rows, rows)]

        return view

    def cols_view(ref):
        cols = ref.shape[2] // 2

        def view(block, part):
            return ref.at[block] if part is None else ref.at[block, :, pl.ds(part * cols, cols)]

        return view

    basis_o = Gather(n, rows_view(gbo), take(), take(), take())
    basis_q = Gather(n, rows_view(gbq), take(), take(), take())
    norm_o = Gather(n, cols_view(no_ref), take(), take(), take())
    norm_q = Gather(n, cols_view(nq_ref), take(), take(), take())
    norm_s = Gather(n, cols_view(gs), take(), take(), take())
    sum_o = Scatter(n, part_o, one_o, mid_o, two_o, total_o, out_o, late_o, take(), take(), take())
    sum_q = Scatter(n, part_q, one_q, mid_q, two_q, total_q, out_q, late_q, take(), take(), take())
    swap_s, swap_r = take()
    share_s, share_r = take()
    pair_s, pair_r = take()
    weight_s, weight_r = take()

    views = []
    for ref, pieces in ((gwq_ref, 2), (gwo_ref, 4)):
        rows = ref.shape[1] // pieces
        for p in range(pieces):
            views.append(lambda b, ref=ref, p=p, rows=rows: ref.at[b, pl.ds(p * rows, rows)])
    weights = Weights(n, views, weight_s, weight_r)

    basis_o.start()
    basis_q.start()
    copies[2].wait()
    copies[3].wait()
    gwq_ref[fs] = wq[...].astype(b16)
    gwo_ref[fs] = wo[...].astype(b16)

    for step in range(1, n):
        basis_o.arrive(step)
        basis_q.arrive(step)
        basis_o.relay(step - 1)
        basis_q.relay(step - 1)
    weights.tick(2)
    basis_o.relay(n - 1)
    weights.tick(1)
    for step in range(n):
        basis_o.finish(step)

    def share(a, f):
        gb, out = ((gbq, hq_ref), (gbo, ho_ref))[a]
        return remote(
            gb.at[rep * n + f], out.at[f, :, own], share_s.at[a, f], share_r.at[a, f], (fs, rep, 1 - tp)
        )

    def share_in(a, f):
        gb, out = ((gbq, hq_ref), (gbo, ho_ref))[a]
        other = pl.ds(pl.multiple_of((1 - tp) * half, half), half)
        return remote(
            gb.at[rep * n + f], out.at[f, :, other], share_s.at[a, f], share_r.at[a, f], (fs, rep, 1 - tp)
        )

    def keep(a):
        gb, out = ((gbq, hq_ref), (gbo, ho_ref))[a]
        for f in range(n):
            out[f, :, own] = gb[rep * n + f]

    def swap(a, core):
        ref = (inq, ino)[a]
        return remote(ref.at[core], ref.at[core], swap_s.at[a], swap_r.at[a], (fs, rep, 1 - tp))

    def project(a):
        x, gb, out = ((xq, gbq, inq), (xo, gbo, ino))[a]
        tile = min(512, x.shape[0])

        def step(t, _):
            span = pl.ds(pl.multiple_of(t * tile, tile), tile)
            value = jnp.dot(x[span, :], gb[...].reshape(-1, half), preferred_element_type=f32)
            out[tp, :, span] = value.T.astype(b16)
            return 0

        lax.fori_loop(0, x.shape[0] // tile, step, 0)
        swap(a, tp).start()

    def norm(a, c, scatter):
        first, second, first_out, second_out, n_out = (
            (fq, sq, nfq_ref, nsq_ref, nq_ref), (fo, so, nfo_ref, nso_ref, no_ref)
        )[a]
        span = pl.ds(c * scatter.width, scatter.width)
        p = scatter.final(c)
        first_next = beta_first * first[:, span] + (1.0 - beta_first) * p
        second_next = beta_second * second[:, span] + (1.0 - beta_second) * p * p
        normed = first_next / jnp.sqrt(second_next)
        first_out[:, span] = first_next
        second_out[:, span] = second_next
        n_out[mine, :, span] = normed.astype(b16)
        square = normed * normed
        rows, cols = square.shape
        square = sum(square[:, k : k + 128] for k in range(0, cols, 128))
        square = sum(square[k : k + 8] for k in range(0, rows, 8))
        slot = pl.ds(a * 128, 128)
        gs[mine, :, slot] = square if c == 0 else gs[mine, :, slot] + square

    copies[4].wait()
    project(1)
    basis_q.relay(n - 1)
    for f in range(n):
        share(1, f).start()
    weights.tick(1)
    copies[5].wait()
    swap(1, 1 - tp).wait_recv()
    for c in range(sum_o.chunks):
        sum_o.compute(c, ino, co)
        sum_o.send(c)
    keep(1)
    weights.tick(1)
    for step in range(n):
        basis_q.finish(step)
    copies[6].wait()
    project(0)
    for f in range(n):
        share(0, f).start()
    weights.tick(1)
    for c in range(2):
        sum_o.middle(c)
    copies[7].wait()
    swap(0, 1 - tp).wait_recv()
    for c in range(sum_q.chunks):
        sum_q.compute(c, inq, cq)
        sum_q.send(c)
    for c in range(2, sum_o.chunks):
        sum_o.middle(c)
    weights.tick(1)
    for copy in copies[8:]:
        copy.wait()
    for c in range(2):
        sum_o.cross(c)
    for c in range(sum_q.chunks):
        sum_q.middle(c)
    for c in range(2, sum_o.chunks):
        sum_o.cross(c)
    keep(0)
    weights.tick(1)
    for c in range(sum_o.chunks):
        norm(1, c, sum_o)
    norm_o.start()
    for c in range(sum_q.chunks):
        sum_q.cross(c)
    for c in range(sum_q.chunks):
        norm(0, c, sum_q)
    norm_q.start()
    norm_s.start()
    norms = (norm_o, norm_q, norm_s)
    for step in range(1, n):
        for g in norms:
            g.arrive(step)
        for g in norms:
            g.relay(step - 1)
    weights.tick(3)
    for g in norms:
        g.relay(n - 1)
    for step in range(n):
        for g in norms:
            g.finish(step)
    tot_ref[0] = sum(gs[b] for b in range(4 * n))
    pair = remote(tot_ref.at[0], tot_ref.at[1], pair_s.at[0], pair_r.at[0], (fs, rep, 1 - tp))
    pair.start()
    weights.finish()
    pair.wait()
    for a in (0, 1):
        swap(a, tp).wait_send()
        for f in range(n):
            share(a, f).wait_send()
            share_in(a, f).wait_recv()
    for g in (basis_o, basis_q, *norms, sum_o, sum_q):
        g.drain()
    weights.sent()


def pairs(*shapes):
    return [DMA(shape) for shape in shapes for _ in (0, 1)]


def advance(n, *args):
    xq, cq, xo, co, wq, wo, bq, bo, fq, sq, fo, so = args
    f32, b16 = jnp.float32, jnp.bfloat16
    shape, vmem = jax.ShapeDtypeStruct, pltpu.VMEM
    rank = bq.shape[1]
    half = rank // 2
    rows = fq.shape[0]
    width_q, width_o = cq.shape[1] // 2, co.shape[1] // 4

    def scatter(chunks, width):
        return [
            vmem((chunks, 4, n * rows, width), b16),
            vmem((chunks, 2, n * rows, width), b16),
            vmem((chunks, n * rows, width), b16),
            vmem((chunks, n * rows, width), b16),
            vmem((chunks, n * rows, width), f32),
            vmem((chunks, n - 1, rows, width), b16),
            vmem((chunks, n - 1, rows, width), b16),
        ]

    slots = 2 * n - 1
    gather = [(2, n - 1), (2, slots), (2, 2, slots)]
    reduce = lambda chunks: [(chunks, 2), (chunks,), (chunks, n - 1)]
    spec = pl.BlockSpec(memory_space=pltpu.VMEM)
    return pl.pallas_call(
        functools.partial(main_kernel, n),
        out_shape=(
            shape((4 * n, rows, cq.shape[1]), b16),
            shape((4 * n, rows, co.shape[1]), b16),
            shape((n, *wq.shape), b16),
            shape((n, *wo.shape), b16),
            shape((n, *bq.shape), b16),
            shape((n, *bo.shape), b16),
            *[shape(a.shape, f32) for a in (fq, sq, fo, so)],
            shape((2, 8, 256), f32),
        ),
        in_specs=[pl.BlockSpec(memory_space=pltpu.HBM)] * 12,
        out_specs=(spec,) * 11,
        scratch_shapes=[vmem(a.shape, a.dtype) for a in (xq, cq, xo, co, wq, wo, fq, sq, fo, so)]
        + [vmem((4 * n, bq.shape[0], half), b16), vmem((4 * n, bo.shape[0], half), b16)]
        + [vmem((2, half, xq.shape[0]), b16), vmem((2, half, xo.shape[0]), b16)]
        + scatter(2, width_q)
        + scatter(4, width_o)
        + [vmem((4 * n, 8, 256), f32), DMA((12,))]
        + pairs(*(gather * 5), *reduce(4), *reduce(2), (2,), (2, n), (1,), (6, 2, n - 1)),
        compiler_params=pltpu.CompilerParams(
            collective_id=0, has_side_effects=True, vmem_limit_bytes=40 * 2**20
        ),
        name="advance",
    )(*[pltpu.with_memory_space_constraint(a, pltpu.HBM) for a in args])


def last_kernel(
    n,
    hq, ho, nq, no, gwq, gwo, nfq, nsq, nfo, nso, tot,
    uq_out, uo_out, nfq_out, nsq_out, nfo_out, nso_out, cq_out, co_out,
    uq, uo, cq, co, sems,
):
    fs = lax.axis_index("fs")
    f32, b16 = jnp.float32, jnp.bfloat16
    copies = []

    def put(src, dst):
        copy = pltpu.make_async_copy(src, dst, sems.at[len(copies)])
        copy.start()
        copies.append(copy)

    for src, dst in ((nfq, nfq_out), (nsq, nsq_out), (nfo, nfo_out), (nso, nso_out)):
        put(src, dst)
    rank = nq.shape[0]
    for a, (rows_ref, normed, weights, u, c, u_hbm, c_hbm) in enumerate(
        ((hq, nq, gwq, uq, cq, uq_out, cq_out), (ho, no, gwo, uo, co, uo_out, co_out))
    ):
        columns = normed.shape[1]
        total = jnp.sum(tot[:, :, a * 128 : (a + 1) * 128], axis=0)
        total = jnp.sum(jnp.sum(total, axis=0, keepdims=True), axis=1, keepdims=True)
        scale = lax.rsqrt(total / (rank * 2 * columns) + small_eps)
        tile = min(256, columns)
        mine = u_hbm.shape[0]
        block = 2 * tile if columns % (2 * tile) == 0 else tile

        for k in range(0, columns, block):

            def step(i, _):
                span = pl.ds(pl.multiple_of(k + i * tile, tile), tile)
                value = scale * jnp.dot(rows_ref[...], normed[:, span], preferred_element_type=f32)
                u[:, span] = value
                c[:, span] = (weights[:, span].astype(f32) - step_rate * value).astype(b16)
                return 0

            lax.fori_loop(0, block // tile, step, 0)
            span = pl.ds(k, block)
            put(u.at[pl.ds(pl.multiple_of(fs * mine, mine), mine), span], u_hbm.at[:, span])
            put(c.at[:, span], c_hbm.at[:, span])
    for copy in copies:
        copy.wait()


def body(n, *args):
    xq, cq, xo, co, wq, wo, bq, bo, fq, sq, fo, so = args
    f32, b16 = jnp.float32, jnp.bfloat16
    rank = bq.shape[1]
    nq, no, gwq, gwo, hq, ho, nfq, nsq, nfo, nso, tot = advance(n, *args)
    shape, vmem = jax.ShapeDtypeStruct, pltpu.VMEM
    flat = lambda a: a.reshape(-1, a.shape[2])
    hq, ho, nq, no, gwq, gwo = [flat(a) for a in (hq, ho, nq, no, gwq, gwo)]
    outs = (
        shape(wq.shape, f32), shape(wo.shape, f32), shape(fq.shape, f32), shape(fq.shape, f32),
        shape(fo.shape, f32), shape(fo.shape, f32), shape(gwq.shape, b16), shape(gwo.shape, b16),
    )
    wide = lambda a: vmem(a.shape, f32)
    spec = pl.BlockSpec(memory_space=pltpu.VMEM)
    return pl.pallas_call(
        functools.partial(last_kernel, n),
        out_shape=outs,
        in_specs=[spec] * 11,
        out_specs=(pl.BlockSpec(memory_space=pl.ANY),) * 8,
        scratch_shapes=[wide(gwq), wide(gwo)]
        + [vmem(gwq.shape, b16), vmem(gwo.shape, b16), DMA((4 + 2 + 2 * (wo.shape[1] // 256),))],
        compiler_params=pltpu.CompilerParams(vmem_limit_bytes=20 * 2**20),
        name="update",
    )(hq, ho, nq, no, gwq, gwo, nfq, nsq, nfo, nso, tot)


def solution(mesh):
    in_specs = (
        P(("fs", "rep"), None),
        P(("fs", "rep"), "tp"),
        P(("fs", "rep"), None),
        P(("fs", "rep"), "tp"),
        P(("rep", "fs"), "tp"),
        P(("rep", "fs"), "tp"),
        P(("rep", "fs"), None),
        P(("rep", "fs"), None),
        P(("rep", "fs"), "tp"),
        P(("rep", "fs"), "tp"),
        P(("rep", "fs"), "tp"),
        P(("rep", "fs"), "tp"),
    )
    out_specs = (
        P(("rep", "fs"), "tp"),
        P(("rep", "fs"), "tp"),
        P(("rep", "fs"), "tp"),
        P(("rep", "fs"), "tp"),
        P(("rep", "fs"), "tp"),
        P(("rep", "fs"), "tp"),
        P("rep", "tp"),
        P("rep", "tp"),
    )
    n = mesh.shape["fs"]
    assert mesh.shape["rep"] == 4 and mesh.shape["tp"] == 2
    return jax.shard_map(functools.partial(body, n), mesh=mesh, in_specs=in_specs, out_specs=out_specs, check_vma=False)
```

time: 177 us -> 130 us (0.73)
  matrix products: 31.9 us -> 0 us
  local copies, waits for them, and re-layouts: 16.1 us -> 0 us
  Pallas kernels: 122 us -> 129 us
  other arithmetic: 4.22 us -> 0 us
    dot_general x6 -> x0, matrix products: 31.9 us -> none  [the longest x2 20.9 us: project(): lax.dot_general(inner, cotangent, (((0,), (0,)), ((), ())), preferred_ele...]
    unnamed x54 -> x0, local copies, waits for them, and re-layouts: 15.5 us -> none
    pallas_call x2, Pallas kernels: 122 us -> 129 us  [the longest x1 124 us: advance(): pl.pallas_call(functools.partial(main_kernel, n), out_shape=(shape((4 * n...]
where the time goes in v1:
time: 130 us
  Pallas kernels  129 us (99%)
    pallas_call x1, Pallas kernels, advance(): pl.pallas_call(functools.partial(main_kernel, n), out_shape=(shape((4 * n...  124 us
    pallas_call x1, Pallas kernels, body(): pl.pallas_call(functools.partial(last_kernel, n), out_shape=outs, in_spec...  4.63 us

profile of v1, /device:TPU:0, one launch (start us, length us, event | category | flops | bytes accessed | tf_op | source)
XLA Modules:
  0.0 129.6 jit_solution(7083515844779883712)
XLA Ops:
  0.6 124.3 %advance.1 = (bf16[16,32,512]{2,1,0:T(8,128)(2,1)S(1)}, bf16[16,32,2048]{2,1,0:T(8,128)(2,1)S(1)}, bf16[4,256,512]{2,1,0:T(8,128)(2,1)S(1)}, bf16[4,128,2048]{2,...) custom-call(bf16[1024,4096]{1,0:T(8,128)(2,1)} %xq_hbm.1, ...), custom_call_target="tpu_custom_call" | custom-call | tf_op jit(solution)/shard_map/advance/pallas_call | solution.py:561
  124.9 4.6 %update.1 = (f32[256,512]{1,0:T(8,128)}, f32[128,2048]{1,0:T(8,128)}, f32[32,512]{1,0:T(8,128)}, f32[32,512]{1,0:T(8,128)}, f32[32,2048]{1,0:T(8,128)}, /*index=...) custom-call(bf16[1024,512]{1,0:T(8,128)(2,1)S(1)} %bitcast.9, bf16[512,512]{1,0:T(8,128)(2,1)S(1)} %bitcast.11, ...), custom_call_target="tpu_custom_call" | custom-call | tf_op jit(solution)/shard_map/update/pallas_call | solution.py:649

commit v2 on v1

v2 whole, which is shorter than its diff:
```python
import functools

import jax
import jax.numpy as jnp
from jax import lax
from jax.experimental import pallas as pl
from jax.experimental.pallas import tpu as pltpu
from jax.sharding import PartitionSpec as P

MESH = pl.DeviceIdType.MESH
DMA = pltpu.SemaphoreType.DMA

beta_first = 0.6
beta_second = 0.8
step_rate = 0.01
small_eps = 1e-06


def here():
    return lax.axis_index("fs"), lax.axis_index("rep"), lax.axis_index("tp")


def flip(rep, bit):
    if bit == 1:
        return rep + 1 - 2 * lax.rem(rep, 2)
    return lax.rem(rep + 2, 4)


def remote(src, dst, send, recv, device):
    return pltpu.make_async_remote_copy(
        src_ref=src, dst_ref=dst, send_sem=send, recv_sem=recv, device_id=device, device_id_type=MESH
    )


def greet(devices):
    barrier = pltpu.get_barrier_semaphore()
    for device in devices:
        pl.semaphore_signal(barrier, inc=1, device_id=device, device_id_type=MESH)
    pl.semaphore_wait(barrier, len(devices))


def when(present, body):
    if present is True:
        body()
    else:
        pl.when(present)(body)


def await_sent(view, sem):
    remote(view, view, sem, sem, here()).wait_send()


def await_heard(view, sem):
    remote(view, view, sem, sem, here()).wait_recv()


class Line:
    def __init__(self, n, view, send, recv):
        self.n, self.view, self.send_sem, self.recv_sem = n, view, send, recv
        self.fs, self.rep, self.tp = here()

    def outgoing(self, step, way):
        fs, n = self.fs, self.n
        if way == 0:
            block, peer = fs - step + 1, fs + 1
            present = jnp.logical_and(block >= 0, peer < n)
        else:
            block, peer = fs + step - 1, fs - 1
            present = jnp.logical_and(block < n, peer >= 0)
        block = lax.rem(block + n, n)
        peer = lax.rem(peer + n, n)
        view = self.view(block)
        return remote(view, view, self.send_sem.at[way], self.recv_sem.at[block], (peer, self.rep, self.tp)), present

    def start(self, step):
        for way in (0, 1):
            copy, present = self.outgoing(step, way)
            when(present, copy.start)

    def arrive(self, step):
        for way in (0, 1):
            block = self.fs - step if way == 0 else self.fs + step
            present = block >= 0 if way == 0 else block < self.n
            block = lax.rem(block + self.n, self.n)
            when(present, lambda: await_heard(self.view(block), self.recv_sem.at[block]))

    def sent(self, many):
        for place in range(self.n):
            right = place + 1 if place < self.n - 1 else 0
            left = self.n - place if place > 0 else 0

            def body():
                for way, count in enumerate((right, left)):
                    if count:
                        await_sent(many(count), self.send_sem.at[way])

            pl.when(self.fs == place)(body)


class Gather:
    bits = ((1, 2), (2, 1))

    def __init__(self, n, view, many, send, line, one, two):
        self.n, self.view, self.many, self.send_sem = n, view, many, send
        self.line, self.one_sem, self.two_sem = line, one, two
        self.fs, self.rep, self.tp = here()

    def slots(self, step):
        if step == 0:
            return [(self.fs, True)]
        left, right = self.fs - step, self.fs + step
        rem = lambda block: lax.rem(block + self.n, self.n)
        return [(rem(left), left >= 0), (rem(right), right < self.n)]

    def each(self, step, action):
        for block, present in self.slots(step):
            when(present, lambda: action(block))

    def one(self, block, half):
        peer = flip(self.rep, self.bits[half][0])
        view = self.view(self.rep * self.n + block, half)
        return remote(view, view, self.send_sem, self.one_sem.at[half, block], (self.fs, peer, self.tp))

    def two(self, block, half, which):
        peer = flip(self.rep, self.bits[half][1])
        held = self.rep if which == 0 else flip(self.rep, self.bits[half][0])
        view = self.view(held * self.n + block, half)
        return remote(view, view, self.send_sem, self.two_sem, (self.fs, peer, self.tp))

    def launch(self, step):
        def action(block):
            for half in (0, 1):
                self.one(block, half).start()
            for half in (0, 1):
                self.two(block, half, 0).start()

        self.each(step, action)

    def start(self):
        own = self.view(self.rep * self.n + self.fs, None)
        for step in range(1, self.n):
            for peer, present in self.slots(step):
                copy = remote(own, own, self.send_sem, self.line.at[self.fs], (peer, self.rep, self.tp))
                when(present, copy.start)
        self.launch(0)

    def arrive(self, step):
        self.each(step, lambda block: await_heard(self.view(self.rep * self.n + block, None), self.line.at[block]))
        self.launch(step)

    def relay(self, step):
        def action(block):
            for half in (0, 1):
                peer = flip(self.rep, self.bits[half][0])
                await_heard(self.view(peer * self.n + block, half), self.one_sem.at[half, block])
                self.two(block, half, 1).start()

        self.each(step, action)

    def events(self):
        n = self.n
        todo = [(self.relay, 0)]
        for step in range(1, n):
            todo.append((self.arrive, step))
            if step >= 2:
                todo.append((self.relay, step - 1))
        return todo + ([(self.relay, n - 1)] if n > 1 else [])

    def finish(self):
        await_heard(self.many(2 * self.n), self.two_sem)

    def drain(self):
        await_sent(self.many(4 * self.n - 1), self.send_sem)


class Scatter:
    def __init__(self, n, part, one, mid, two, total, out, late, send, one_sem, two_sem, line_sem):
        self.n, self.part, self.heard, self.mid_ref, self.two = n, part, one, mid, two
        self.total, self.out, self.late = total, out, late
        self.send_sem, self.one_sem, self.two_sem, self.line_sem = send, one_sem, two_sem, line_sem
        self.fs, self.rep, self.tp = here()
        self.chunks, _, group, self.width = part.shape
        self.rows = group // n

    def peers(self, c):
        first, second = ((1, 2), (2, 1))[c % 2]
        return flip(self.rep, first), flip(self.rep, second), second

    def compute(self, c, inner, cotangent):
        tile = min(256, self.width)
        rank = inner.shape[0] * inner.shape[1]

        def step(i, _):
            span = pl.ds(pl.multiple_of(c * self.width + i * tile, tile), tile)
            value = jnp.dot(
                inner[...].reshape(rank, -1), cotangent[:, span], preferred_element_type=jnp.float32
            )
            here_span = pl.ds(pl.multiple_of(i * tile, tile), tile)
            self.part[c, :, :, here_span] = value.astype(jnp.bfloat16).reshape(4, -1, tile)
            return 0

        lax.fori_loop(0, self.width // tile, step, 0)

    def send(self, c):
        near, _, second = self.peers(c)
        for slot, group in ((1, flip(near, second)), (0, near)):
            remote(
                self.part.at[c, group], self.heard.at[c, slot], self.send_sem.at[0], self.one_sem.at[c],
                (self.fs, near, self.tp),
            ).start()

    def middle(self, c):
        f32 = jnp.float32
        _, far, _ = self.peers(c)
        await_heard(self.heard.at[c], self.one_sem.at[c])
        value = self.part[c, far].astype(f32) + self.heard[c, 1].astype(f32)
        self.mid_ref[c] = value.astype(jnp.bfloat16)
        remote(
            self.mid_ref.at[c], self.two.at[c], self.send_sem.at[1], self.two_sem.at[c], (self.fs, far, self.tp)
        ).start()
        self.total[c] = self.part[c, self.rep].astype(f32) + self.heard[c, 0].astype(f32)

    def rows_of(self, c, f):
        span = pl.ds(pl.multiple_of(f * self.rows, self.rows), self.rows)
        return self.total[c, span, :] + self.two[c, span, :].astype(jnp.float32)

    def cross(self, c):
        await_heard(self.two.at[c], self.two_sem.at[c])
        for j in range(1, self.n):
            f = lax.rem(self.fs + j, self.n)
            self.out[c, j - 1] = self.rows_of(c, f).astype(jnp.bfloat16)
            remote(
                self.out.at[c, j - 1], self.late.at[c, j - 1], self.send_sem.at[2], self.line_sem.at[c],
                (f, self.rep, self.tp),
            ).start()

    def final(self, c):
        value = self.rows_of(c, self.fs)
        await_heard(self.late.at[c], self.line_sem.at[c])
        for j in range(1, self.n):
            value = value + self.late[c, j - 1].astype(jnp.float32)
        return value

    def drain(self):
        await_sent(self.heard, self.send_sem.at[0])
        await_sent(self.mid_ref, self.send_sem.at[1])
        await_sent(self.out, self.send_sem.at[2])


class Weights:
    def __init__(self, n, views, many, send, recv):
        self.lines = [Line(n, v, send.at[i], recv.at[i]) for i, v in enumerate(views)]
        self.n, self.many = n, many
        self.todo = [(step, line) for step in range(1, n) for line in self.lines]

    def tick(self, count):
        for _ in range(count):
            if self.todo:
                step, line = self.todo.pop(0)
                if step > 1:
                    line.arrive(step - 1)
                line.start(step)

    def finish(self):
        self.tick(len(self.todo))
        for line in self.lines:
            line.arrive(self.n - 1)

    def sent(self):
        for line, many in zip(self.lines, self.many):
            line.sent(many)


def main_kernel(
    n,
    xq_hbm, cq_hbm, xo_hbm, co_hbm, wq_hbm, wo_hbm, bq_hbm, bo_hbm, fq_hbm, sq_hbm, fo_hbm, so_hbm,
    nq_ref, no_ref, gwq_ref, gwo_ref, hq_ref, ho_ref, nfq_ref, nsq_ref, nfo_ref, nso_ref, tot_ref,
    xq, cq, xo, co, wq, wo, fq, sq, fo, so, gbq, gbo, inq, ino,
    part_q, one_q, mid_q, two_q, total_q, out_q, late_q,
    part_o, one_o, mid_o, two_o, total_o, out_o, late_o,
    gs, local, *sems,
):
    fs, rep, tp = here()
    mine = rep * n + fs
    f32, b16 = jnp.float32, jnp.bfloat16
    sems = list(sems)
    take = lambda count: [sems.pop(0) for _ in range(count)]

    half = bq_hbm.shape[1] // 2
    own = pl.ds(pl.multiple_of(tp * half, half), half)
    copies = [
        pltpu.make_async_copy(src, dst, local.at[i])
        for i, (src, dst) in enumerate(
            [
                (bo_hbm.at[:, own], gbo.at[mine]), (bq_hbm.at[:, own], gbq.at[mine]),
                (wq_hbm, wq), (wo_hbm, wo), (xo_hbm, xo), (co_hbm, co), (xq_hbm, xq), (cq_hbm, cq),
                (fo_hbm, fo), (so_hbm, so), (fq_hbm, fq), (sq_hbm, sq),
            ]
        )
    ]
    for copy in copies:
        copy.start()
    copies[0].wait()
    copies[1].wait()
    peers = [(lax.rem(fs + k, n), rep, tp) for k in range(1, n)]
    peers += [(fs, flip(rep, bit), tp) for bit in (1, 2)] + [(fs, rep, 1 - tp)]
    greet(peers)

    def rows_view(ref):
        rows = ref.shape[1] // 2

        def view(block, part):
            return ref.at[block] if part is None else ref.at[block, pl.ds(part * rows, rows)]

        return view, lambda count: ref.at[pl.ds(0, count)]

    def cols_view(ref, index=0, count=1):
        cols = ref.shape[2] // (2 * count)

        def view(block, part):
            start, size = (0, 2 * cols) if part is None else (part * cols, cols)
            return ref.at[block, :, pl.ds(index * 2 * cols + start, size)]

        return view, lambda k: ref.at[pl.ds(0, k), :, pl.ds(index * 2 * cols, 2 * cols)]

    basis_o = Gather(n, *rows_view(gbo), *take(4))
    basis_q = Gather(n, *rows_view(gbq), *take(4))
    norm_o = [Gather(n, *cols_view(no_ref, i, 2), *take(4)) for i in range(2)]
    norm_q = Gather(n, *cols_view(nq_ref), *take(4))
    norm_s = Gather(n, *cols_view(gs), *take(4))
    sum_o = Scatter(n, part_o, one_o, mid_o, two_o, total_o, out_o, late_o, *take(4))
    sum_q = Scatter(n, part_q, one_q, mid_q, two_q, total_q, out_q, late_q, *take(4))
    swap_s, swap_r, share_s, share_r, pair_s, pair_r, weight_s, weight_r = take(8)

    views, many = [], []
    for ref, pieces in ((gwq_ref, 2), (gwo_ref, 4)):
        rows = ref.shape[1] // pieces
        for p in range(pieces):
            views.append(lambda b, ref=ref, p=p, rows=rows: ref.at[b, pl.ds(p * rows, rows)])
            many.append(lambda k, ref=ref, p=p, rows=rows: ref.at[pl.ds(0, k), pl.ds(p * rows, rows)])
    weights = Weights(n, views, many, weight_s, weight_r)

    basis_o.start()
    basis_q.start()
    copies[2].wait()
    copies[3].wait()
    gwq_ref[fs] = wq[...].astype(b16)
    gwo_ref[fs] = wo[...].astype(b16)

    queue = basis_q.events()

    def turn(count):
        for _ in range(count):
            if queue:
                action, step = queue.pop(0)
                action(step)

    for step in range(1, n):
        basis_o.arrive(step)
        basis_o.relay(step - 1)
        if step == 2:
            turn(1)
    basis_o.relay(n - 1)
    turn(2)
    basis_o.finish()

    def share(a):
        gb, out = ((gbq, hq_ref), (gbo, ho_ref))[a]
        for f in range(n):
            view = out.at[f, :, own]
            remote(gb.at[rep * n + f], view, share_s.at[a], share_r.at[a], (fs, rep, 1 - tp)).start()

    def shared(a):
        gb, out = ((gbq, hq_ref), (gbo, ho_ref))[a]
        other = pl.ds(pl.multiple_of((1 - tp) * half, half), half)
        await_heard(out.at[:, :, other], share_r.at[a])
        await_sent(gb.at[pl.ds(0, n)], share_s.at[a])

    def keep(a):
        gb, out = ((gbq, hq_ref), (gbo, ho_ref))[a]
        for f in range(n):
            out[f, :, own] = gb[rep * n + f]

    tokens = xq.shape[0]
    tile = min(512, tokens)

    def swap(a, t):
        ref = (inq, ino)[a]
        view = ref.at[tp, :, pl.ds(pl.multiple_of(t * tile, tile), tile)]
        return remote(view, view, swap_s.at[a], swap_r.at[a], (fs, rep, 1 - tp))

    def project(a):
        x, gb, out = ((xq, gbq, inq), (xo, gbo, ino))[a]

        def step(t, _):
            span = pl.ds(pl.multiple_of(t * tile, tile), tile)
            value = jnp.dot(x[span, :], gb[...].reshape(-1, half), preferred_element_type=f32)
            out[tp, :, span] = value.T.astype(b16)
            swap(a, t).start()
            return 0

        lax.fori_loop(0, tokens // tile, step, 0)

    def swapped(a):
        await_heard((inq, ino)[a].at[1 - tp], swap_r.at[a])

    def norm(a, c, scatter):
        first, second, first_out, second_out, n_out = (
            (fq, sq, nfq_ref, nsq_ref, nq_ref), (fo, so, nfo_ref, nso_ref, no_ref)
        )[a]
        span = pl.ds(c * scatter.width, scatter.width)
        p = scatter.final(c)
        first_next = beta_first * first[:, span] + (1.0 - beta_first) * p
        second_next = beta_second * second[:, span] + (1.0 - beta_second) * p * p
        normed = first_next / jnp.sqrt(second_next)
        first_out[:, span] = first_next
        second_out[:, span] = second_next
        n_out[mine, :, span] = normed.astype(b16)
        square = normed * normed
        rows, cols = square.shape
        square = sum(square[:, k : k + 128] for k in range(0, cols, 128))
        square = sum(square[k : k + 8] for k in range(0, rows, 8))
        slot = pl.ds(a * 128, 128)
        gs[mine, :, slot] = square if c == 0 else gs[mine, :, slot] + square

    copies[4].wait()
    project(1)
    turn(2)
    weights.tick(2)
    copies[5].wait()
    swapped(1)
    chunks = sum_o.chunks
    quarter = chunks // 4
    for c in range(chunks):
        sum_o.compute(c, ino, co)
        if c < 2 * quarter:
            sum_o.send(c)
        if c == 2 * quarter:
            turn(1)
            weights.tick(2)
    turn(len(queue))
    keep(1)
    weights.tick(2)

    def group(i):
        return range(i * quarter, (i + 1) * quarter)

    for c in group(0):
        sum_o.middle(c)
    for c in group(2):
        sum_o.send(c)
    for c in group(1):
        sum_o.middle(c)
    for c in group(3):
        sum_o.send(c)
    for c in group(0):
        sum_o.cross(c)
    for copy in copies[6:]:
        copy.wait()
    for c in group(2):
        sum_o.middle(c)
    for c in group(1):
        sum_o.cross(c)
    weights.tick(1)
    basis_q.finish()
    project(0)
    for c in group(3):
        sum_o.middle(c)
    for c in group(2):
        sum_o.cross(c)
    swapped(0)
    for c in range(sum_q.chunks):
        sum_q.compute(c, inq, cq)
        sum_q.send(c)
    for c in group(3):
        sum_o.cross(c)
    for i in (0, 1):
        for c in group(i):
            norm(1, c, sum_o)
    norm_o[0].start()
    for c in range(sum_q.chunks):
        sum_q.middle(c)
    for c in range(sum_q.chunks):
        sum_q.cross(c)
    for i in (2, 3):
        for c in group(i):
            norm(1, c, sum_o)
    norm_o[1].start()
    queue.extend(norm_o[0].events())
    turn(2)
    share(1)
    share(0)
    keep(0)
    for c in range(sum_q.chunks):
        norm(0, c, sum_q)
    norm_q.start()
    norm_s.start()
    weights.tick(3)
    later = [*zip(norm_o[1].events(), norm_q.events(), norm_s.events())]
    for k, steps in enumerate(later):
        turn(1)
        for action, step in steps:
            action(step)
        weights.tick(1)
    turn(len(queue))
    norms = (*norm_o, norm_q, norm_s)
    for g in norms:
        g.finish()
    tot_ref[0] = sum(gs[b] for b in range(4 * n))
    pair = remote(tot_ref.at[0], tot_ref.at[1], pair_s.at[0], pair_r.at[0], (fs, rep, 1 - tp))
    pair.start()
    weights.finish()
    pair.wait()
    for a in (0, 1):
        await_sent((inq, ino)[a].at[tp], swap_s.at[a])
        shared(a)
    for g in (basis_o, basis_q, *norms, sum_o, sum_q):
        g.drain()
    weights.sent()


def advance(n, *args):
    xq, cq, xo, co, wq, wo, bq, bo, fq, sq, fo, so = args
    f32, b16 = jnp.float32, jnp.bfloat16
    shape, vmem = jax.ShapeDtypeStruct, pltpu.VMEM
    rank = bq.shape[1]
    half = rank // 2
    rows = fq.shape[0]
    width_q, width_o = cq.shape[1] // 2, co.shape[1] // 8

    def scatter(chunks, width):
        return [
            vmem((chunks, 4, n * rows, width), b16),
            vmem((chunks, 2, n * rows, width), b16),
            vmem((chunks, n * rows, width), b16),
            vmem((chunks, n * rows, width), b16),
            vmem((chunks, n * rows, width), f32),
            vmem((chunks, n - 1, rows, width), b16),
            vmem((chunks, n - 1, rows, width), b16),
        ]

    gather = [(), (n,), (2, n), ()]
    reduce = lambda chunks: [(3,), (chunks,), (chunks,), (chunks,)]
    shapes = gather * 6 + reduce(8) + reduce(2) + [(2,), (2,), (2,), (2,), (1,), (1,), (6, 2), (6, n)]
    spec = pl.BlockSpec(memory_space=pltpu.VMEM)
    return pl.pallas_call(
        functools.partial(main_kernel, n),
        out_shape=(
            shape((4 * n, rows, cq.shape[1]), b16),
            shape((4 * n, rows, co.shape[1]), b16),
            shape((n, *wq.shape), b16),
            shape((n, *wo.shape), b16),
            shape((n, *bq.shape), b16),
            shape((n, *bo.shape), b16),
            *[shape(a.shape, f32) for a in (fq, sq, fo, so)],
            shape((2, 8, 256), f32),
        ),
        in_specs=[pl.BlockSpec(memory_space=pltpu.HBM)] * 12,
        out_specs=(spec,) * 11,
        scratch_shapes=[vmem(a.shape, a.dtype) for a in (xq, cq, xo, co, wq, wo, fq, sq, fo, so)]
        + [vmem((4 * n, bq.shape[0], half), b16), vmem((4 * n, bo.shape[0], half), b16)]
        + [vmem((2, half, xq.shape[0]), b16), vmem((2, half, xo.shape[0]), b16)]
        + scatter(2, width_q)
        + scatter(8, width_o)
        + [vmem((4 * n, 8, 256), f32), DMA((12,))]
        + [DMA(a) if a else DMA for a in shapes],
        compiler_params=pltpu.CompilerParams(
            collective_id=0, has_side_effects=True, vmem_limit_bytes=40 * 2**20
        ),
        name="advance",
    )(*[pltpu.with_memory_space_constraint(a, pltpu.HBM) for a in args])


def last_kernel(
    n,
    hq, ho, nq, no, gwq, gwo, nfq, nsq, nfo, nso, tot,
    uq_out, uo_out, nfq_out, nsq_out, nfo_out, nso_out, cq_out, co_out,
    uq, uo, cq, co, sems,
):
    fs = lax.axis_index("fs")
    f32, b16 = jnp.float32, jnp.bfloat16
    copies = []

    def put(src, dst):
        copy = pltpu.make_async_copy(src, dst, sems.at[len(copies)])
        copy.start()
        copies.append(copy)

    for src, dst in ((nfq, nfq_out), (nsq, nsq_out), (nfo, nfo_out), (nso, nso_out)):
        put(src, dst)
    rank = nq.shape[0]
    for a, (rows_ref, normed, weights, u, c, u_hbm, c_hbm) in enumerate(
        ((hq, nq, gwq, uq, cq, uq_out, cq_out), (ho, no, gwo, uo, co, uo_out, co_out))
    ):
        columns = normed.shape[1]
        total = jnp.sum(tot[:, :, a * 128 : (a + 1) * 128], axis=0)
        total = jnp.sum(jnp.sum(total, axis=0, keepdims=True), axis=1, keepdims=True)
        scale = lax.rsqrt(total / (rank * 2 * columns) + small_eps)
        tile = min(256, columns)
        mine = u_hbm.shape[0]
        block = 2 * tile if columns % (2 * tile) == 0 else tile

        for k in range(0, columns, block):

            def step(i, _):
                span = pl.ds(pl.multiple_of(k + i * tile, tile), tile)
                value = scale * jnp.dot(rows_ref[...], normed[:, span], preferred_element_type=f32)
                u[:, span] = value
                c[:, span] = (weights[:, span].astype(f32) - step_rate * value).astype(b16)
                return 0

            lax.fori_loop(0, block // tile, step, 0)
            span = pl.ds(k, block)
            put(u.at[pl.ds(pl.multiple_of(fs * mine, mine), mine), span], u_hbm.at[:, span])
            put(c.at[:, span], c_hbm.at[:, span])
    for copy in copies:
        copy.wait()


def body(n, *args):
    xq, cq, xo, co, wq, wo, bq, bo, fq, sq, fo, so = args
    f32, b16 = jnp.float32, jnp.bfloat16
    rank = bq.shape[1]
    nq, no, gwq, gwo, hq, ho, nfq, nsq, nfo, nso, tot = advance(n, *args)
    shape, vmem = jax.ShapeDtypeStruct, pltpu.VMEM
    flat = lambda a: a.reshape(-1, a.shape[2])
    hq, ho, nq, no, gwq, gwo = [flat(a) for a in (hq, ho, nq, no, gwq, gwo)]
    outs = (
        shape(wq.shape, f32), shape(wo.shape, f32), shape(fq.shape, f32), shape(fq.shape, f32),
        shape(fo.shape, f32), shape(fo.shape, f32), shape(gwq.shape, b16), shape(gwo.shape, b16),
    )
    wide = lambda a: vmem(a.shape, f32)
    spec = pl.BlockSpec(memory_space=pltpu.VMEM)
    return pl.pallas_call(
        functools.partial(last_kernel, n),
        out_shape=outs,
        in_specs=[spec] * 11,
        out_specs=(pl.BlockSpec(memory_space=pl.ANY),) * 8,
        scratch_shapes=[wide(gwq), wide(gwo)]
        + [vmem(gwq.shape, b16), vmem(gwo.shape, b16), DMA((4 + 2 + 2 * (wo.shape[1] // 256),))],
        compiler_params=pltpu.CompilerParams(vmem_limit_bytes=20 * 2**20),
        name="update",
    )(hq, ho, nq, no, gwq, gwo, nfq, nsq, nfo, nso, tot)


def solution(mesh):
    in_specs = (
        P(("fs", "rep"), None),
        P(("fs", "rep"), "tp"),
        P(("fs", "rep"), None),
        P(("fs", "rep"), "tp"),
        P(("rep", "fs"), "tp"),
        P(("rep", "fs"), "tp"),
        P(("rep", "fs"), None),
        P(("rep", "fs"), None),
        P(("rep", "fs"), "tp"),
        P(("rep", "fs"), "tp"),
        P(("rep", "fs"), "tp"),
        P(("rep", "fs"), "tp"),
    )
    out_specs = (
        P(("rep", "fs"), "tp"),
        P(("rep", "fs"), "tp"),
        P(("rep", "fs"), "tp"),
        P(("rep", "fs"), "tp"),
        P(("rep", "fs"), "tp"),
        P(("rep", "fs"), "tp"),
        P("rep", "tp"),
        P("rep", "tp"),
    )
    n = mesh.shape["fs"]
    assert mesh.shape["rep"] == 4 and mesh.shape["tp"] == 2
    return jax.shard_map(functools.partial(body, n), mesh=mesh, in_specs=in_specs, out_specs=out_specs, check_vma=False)
```

time: 130 us -> 111 us (0.85)
  Pallas kernels: 129 us -> 110 us
    pallas_call x1, Pallas kernels: 124 us -> 106 us  [advance(): pl.pallas_call(functools.partial(main_kernel, n), out_shape=(shape((4 * n...]
where the time goes in v2:
time: 111 us
  Pallas kernels  110 us (99%)
    pallas_call x1, Pallas kernels, advance(): pl.pallas_call(functools.partial(main_kernel, n), out_shape=(shape((4 * n...  106 us
    pallas_call x1, Pallas kernels, body(): pl.pallas_call(functools.partial(last_kernel, n), out_shape=outs, in_spec...  4.63 us

profile of v2, /device:TPU:0, one launch (start us, length us, event | category | flops | bytes accessed | tf_op | source)
XLA Modules:
  0.0 111.0 jit_solution(16250107177498876958)
XLA Ops:
  0.6 105.7 %advance.1 = (bf16[16,32,512]{2,1,0:T(8,128)(2,1)S(1)}, bf16[16,32,2048]{2,1,0:T(8,128)(2,1)S(1)}, bf16[4,256,512]{2,1,0:T(8,128)(2,1)S(1)}, bf16[4,128,2048]{2,...) custom-call(bf16[1024,4096]{1,0:T(8,128)(2,1)} %xq_hbm.1, ...), custom_call_target="tpu_custom_call" | custom-call | tf_op jit(solution)/shard_map/advance/pallas_call | solution.py:546
  106.4 4.6 %update.1 = (f32[256,512]{1,0:T(8,128)}, f32[128,2048]{1,0:T(8,128)}, f32[32,512]{1,0:T(8,128)}, f32[32,512]{1,0:T(8,128)}, f32[32,2048]{1,0:T(8,128)}, /*index=...) custom-call(bf16[1024,512]{1,0:T(8,128)(2,1)S(1)} %bitcast.9, bf16[512,512]{1,0:T(8,128)(2,1)S(1)} %bitcast.11, ...), custom_call_target="tpu_custom_call" | custom-call | tf_op jit(solution)/shard_map/update/pallas_call | solution.py:634

commit v3 on v2

--- a/solution.py
+++ b/solution.py
@@ -220,31 +220,68 @@
         ).start()
         self.total[c] = self.part[c, self.rep].astype(f32) + self.heard[c, 0].astype(f32)
 
-    def rows_of(self, c, f):
-        span = pl.ds(pl.multiple_of(f * self.rows, self.rows), self.rows)
-        return self.total[c, span, :] + self.two[c, span, :].astype(jnp.float32)
+    def sums(self, c, rows):
+        return self.total[c, rows, :] + self.two[c, rows, :].astype(jnp.float32)
+
+    def stream(self, c, place, way, heard):
+        n, r = self.n, self.rows
+        rows = pl.ds((place + 1) * r, (n - 1 - place) * r) if way == 0 else pl.ds(0, place * r)
+        value = self.sums(c, rows)
+        if heard:
+            value = value + self.late[c, way, rows, :].astype(jnp.float32)
+        self.out[c, rows, :] = value.astype(jnp.bfloat16)
+        peer = (place + 1 if way == 0 else place - 1, self.rep, self.tp)
+        remote(
+            self.out.at[c, rows], self.late.at[c, way, rows], self.send_sem.at[2 + way],
+            self.line_sem.at[c, way], peer,
+        ).start()
+
+    def hear(self, c, place, way):
+        n, r = self.n, self.rows
+        rows = pl.ds(place * r, (n - place) * r) if way == 0 else pl.ds(0, (place + 1) * r)
+        await_heard(self.late.at[c, way, rows], self.line_sem.at[c, way])
 
     def cross(self, c):
         await_heard(self.two.at[c], self.two_sem.at[c])
-        for j in range(1, self.n):
-            f = lax.rem(self.fs + j, self.n)
-            self.out[c, j - 1] = self.rows_of(c, f).astype(jnp.bfloat16)
-            remote(
-                self.out.at[c, j - 1], self.late.at[c, j - 1], self.send_sem.at[2], self.line_sem.at[c],
-                (f, self.rep, self.tp),
-            ).start()
+        for place, way in ((0, 0), (self.n - 1, 1)):
+            pl.when(self.fs == place)(lambda: self.stream(c, place, way, False))
+
+    def onward(self, c, turn):
+        for place in range(1, self.n - 1):
+            way = turn if 2 * place < self.n else 1 - turn
+
+            def body():
+                self.hear(c, place, way)
+                self.stream(c, place, way, True)
+
+            pl.when(self.fs == place)(body)
 
     def final(self, c):
-        value = self.rows_of(c, self.fs)
-        await_heard(self.late.at[c], self.line_sem.at[c])
-        for j in range(1, self.n):
-            value = value + self.late[c, j - 1].astype(jnp.float32)
-        return value
+        n, r = self.n, self.rows
+        for place, way in ((0, 1), (n - 1, 0)):
+            pl.when(self.fs == place)(lambda: self.hear(c, place, way))
+        own = pl.ds(pl.multiple_of(self.fs * r, r), r)
+        self.total[c, own, :] = self.sums(c, own)
+        for way, present in ((0, self.fs > 0), (1, self.fs < n - 1)):
+
+            def body():
+                self.total[c, own, :] = self.total[c, own, :] + self.late[c, way, own, :].astype(jnp.float32)
+
+            pl.when(present)(body)
+        return self.total[c, own, :]
 
     def drain(self):
         await_sent(self.heard, self.send_sem.at[0])
         await_sent(self.mid_ref, self.send_sem.at[1])
-        await_sent(self.out, self.send_sem.at[2])
+        n, r = self.n, self.rows
+        for place in range(n):
+
+            def body():
+                for way, count in ((0, n - 1 - place), (1, place)):
+                    if count:
+                        await_sent(self.out.at[:, pl.ds(0, count * r)], self.send_sem.at[2 + way])
+
+            pl.when(self.fs == place)(body)
 
 
 class Weights:
@@ -269,6 +306,10 @@
     def sent(self):
         for line, many in zip(self.lines, self.many):
             line.sent(many)
+
+
+def pieces_of(*refs):
+    return [min(most, ref.shape[-2] // 8) for most, ref in zip((4, 8), refs)]
 
 
 def main_kernel(
@@ -333,7 +374,7 @@
     swap_s, swap_r, share_s, share_r, pair_s, pair_r, weight_s, weight_r = take(8)
 
     views, many = [], []
-    for ref, pieces in ((gwq_ref, 2), (gwo_ref, 4)):
+    for ref, pieces in zip((gwq_ref, gwo_ref), pieces_of(gwq_ref, gwo_ref)):
         rows = ref.shape[1] // pieces
         for p in range(pieces):
             views.append(lambda b, ref=ref, p=p, rows=rows: ref.at[b, pl.ds(p * rows, rows)])
@@ -361,7 +402,7 @@
         if step == 2:
             turn(1)
     basis_o.relay(n - 1)
-    turn(2)
+    turn(1)
     basis_o.finish()
 
     def share(a):
@@ -425,8 +466,8 @@
 
     copies[4].wait()
     project(1)
-    turn(2)
-    weights.tick(2)
+    turn(3)
+    weights.tick(6)
     copies[5].wait()
     swapped(1)
     chunks = sum_o.chunks
@@ -437,10 +478,10 @@
             sum_o.send(c)
         if c == 2 * quarter:
             turn(1)
-            weights.tick(2)
+            weights.tick(4)
     turn(len(queue))
     keep(1)
-    weights.tick(2)
+    weights.tick(4)
 
     def group(i):
         return range(i * quarter, (i + 1) * quarter)
@@ -453,56 +494,80 @@
         sum_o.middle(c)
     for c in group(3):
         sum_o.send(c)
+    weights.tick(2)
+    for copy in copies[6:]:
+        copy.wait()
+    basis_q.finish()
+    project(0)
     for c in group(0):
         sum_o.cross(c)
-    for copy in copies[6:]:
-        copy.wait()
     for c in group(2):
         sum_o.middle(c)
-    for c in group(1):
-        sum_o.cross(c)
-    weights.tick(1)
-    basis_q.finish()
-    project(0)
-    for c in group(3):
-        sum_o.middle(c)
-    for c in group(2):
-        sum_o.cross(c)
     swapped(0)
     for c in range(sum_q.chunks):
         sum_q.compute(c, inq, cq)
         sum_q.send(c)
+    def cross(i):
+        for c in group(i):
+            sum_o.cross(c)
+
+    def onward(i, turn):
+        for c in group(i):
+            sum_o.onward(c, turn)
+
+    def both(i):
+        for k in (i, i + 1):
+            for c in group(k):
+                norm(1, c, sum_o)
+
+    cross(1)
+    onward(0, 0)
+    weights.tick(1)
     for c in group(3):
-        sum_o.cross(c)
-    for i in (0, 1):
-        for c in group(i):
-            norm(1, c, sum_o)
-    norm_o[0].start()
+        sum_o.middle(c)
+    cross(2)
+    onward(1, 0)
+    onward(0, 1)
+    weights.tick(1)
+    cross(3)
+    onward(2, 0)
+    onward(1, 1)
+    weights.tick(1)
     for c in range(sum_q.chunks):
         sum_q.middle(c)
+    onward(3, 0)
+    onward(2, 1)
+    weights.tick(1)
     for c in range(sum_q.chunks):
         sum_q.cross(c)
-    for i in (2, 3):
-        for c in group(i):
-            norm(1, c, sum_o)
+    both(0)
+    norm_o[0].start()
+    queue.extend(norm_o[0].events())
+    onward(3, 1)
+    for c in range(sum_q.chunks):
+        sum_q.onward(c, 0)
+    both(2)
     norm_o[1].start()
-    queue.extend(norm_o[0].events())
+    weights.tick(2)
+    for c in range(sum_q.chunks):
+        sum_q.onward(c, 1)
     turn(2)
-    share(1)
-    share(0)
-    keep(0)
+    weights.tick(2)
     for c in range(sum_q.chunks):
         norm(0, c, sum_q)
     norm_q.start()
     norm_s.start()
-    weights.tick(3)
+    weights.tick(4)
+    turn(1)
+    share(1)
+    share(0)
+    keep(0)
+    turn(len(queue))
     later = [*zip(norm_o[1].events(), norm_q.events(), norm_s.events())]
     for k, steps in enumerate(later):
-        turn(1)
         for action, step in steps:
             action(step)
-        weights.tick(1)
-    turn(len(queue))
+        weights.tick(2)
     norms = (*norm_o, norm_q, norm_s)
     for g in norms:
         g.finish()
@@ -535,13 +600,14 @@
             vmem((chunks, n * rows, width), b16),
             vmem((chunks, n * rows, width), b16),
             vmem((chunks, n * rows, width), f32),
-            vmem((chunks, n - 1, rows, width), b16),
-            vmem((chunks, n - 1, rows, width), b16),
+            vmem((chunks, n * rows, width), b16),
+            vmem((chunks, 2, n * rows, width), b16),
         ]
 
+    pieces = sum(pieces_of(wq, wo))
     gather = [(), (n,), (2, n), ()]
-    reduce = lambda chunks: [(3,), (chunks,), (chunks,), (chunks,)]
-    shapes = gather * 6 + reduce(8) + reduce(2) + [(2,), (2,), (2,), (2,), (1,), (1,), (6, 2), (6, n)]
+    reduce = lambda chunks: [(4,), (chunks,), (chunks,), (chunks, 2)]
+    shapes = gather * 6 + reduce(8) + reduce(2) + [(2,), (2,), (2,), (2,), (1,), (1,), (pieces, 2), (pieces, n)]
     spec = pl.BlockSpec(memory_space=pltpu.VMEM)
     return pl.pallas_call(
         functools.partial(main_kernel, n),

time: 111 us -> 105 us (0.946)
  Pallas kernels: 110 us -> 104 us
    pallas_call x1, Pallas kernels: 106 us -> 99.8 us  [advance(): pl.pallas_call(functools.partial(main_kernel, n), out_shape=(shape((4 * n...]
where the time goes in v3:
time: 105 us
  Pallas kernels  104 us (99%)
    pallas_call x1, Pallas kernels, advance(): pl.pallas_call(functools.partial(main_kernel, n), out_shape=(shape((4 * n...  99.8 us
    pallas_call x1, Pallas kernels, body(): pl.pallas_call(functools.partial(last_kernel, n), out_shape=outs, in_spec...  4.63 us

profile of v3, /device:TPU:0, one launch (start us, length us, event | category | flops | bytes accessed | tf_op | source)
XLA Modules:
  0.0 105.1 jit_solution(14951082068178728618)
XLA Ops:
  0.6 99.8 %advance.1 = (bf16[16,32,512]{2,1,0:T(8,128)(2,1)S(1)}, bf16[16,32,2048]{2,1,0:T(8,128)(2,1)S(1)}, bf16[4,256,512]{2,1,0:T(8,128)(2,1)S(1)}, bf16[4,128,2048]{2,...) custom-call(bf16[1024,4096]{1,0:T(8,128)(2,1)} %xq_hbm.1, ...), custom_call_target="tpu_custom_call" | custom-call | tf_op jit(solution)/shard_map/advance/pallas_call | solution.py:612
  100.5 4.6 %update.1 = (f32[256,512]{1,0:T(8,128)}, f32[128,2048]{1,0:T(8,128)}, f32[32,512]{1,0:T(8,128)}, f32[32,512]{1,0:T(8,128)}, f32[32,2048]{1,0:T(8,128)}, /*index=...) custom-call(bf16[1024,512]{1,0:T(8,128)(2,1)S(1)} %bitcast.9, bf16[512,512]{1,0:T(8,128)(2,1)S(1)} %bitcast.11, ...), custom_call_target="tpu_custom_call" | custom-call | tf_op jit(solution)/shard_map/update/pallas_call | solution.py:700

commit v4 on v3

--- a/solution.py
+++ b/solution.py
@@ -72,9 +72,12 @@
         view = self.view(block)
         return remote(view, view, self.send_sem.at[way], self.recv_sem.at[block], (peer, self.rep, self.tp)), present
 
-    def start(self, step):
+    def start(self, step, part=None):
         for way in (0, 1):
             copy, present = self.outgoing(step, way)
+            if part is not None:
+                right = 2 * self.fs >= self.n if (way == 0) == (part == 0) else 2 * self.fs < self.n
+                present = jnp.logical_and(present, right)
             when(present, copy.start)
 
     def arrive(self, step):
@@ -100,7 +103,8 @@
 class Gather:
     bits = ((1, 2), (2, 1))
 
-    def __init__(self, n, view, many, send, line, one, two):
+    def __init__(self, n, far, view, many, send, line, one, two):
+        self.far = far and n > 3
         self.n, self.view, self.many, self.send_sem = n, view, many, send
         self.line, self.one_sem, self.two_sem = line, one, two
         self.fs, self.rep, self.tp = here()
@@ -137,15 +141,20 @@
         self.each(step, action)
 
     def start(self):
-        own = self.view(self.rep * self.n + self.fs, None)
-        for step in range(1, self.n):
+        for step in range(1, self.n - 1 if self.far else self.n):
             for peer, present in self.slots(step):
-                copy = remote(own, own, self.send_sem, self.line.at[self.fs], (peer, self.rep, self.tp))
-                when(present, copy.start)
+                when(present, lambda: self.along(self.fs, peer))
         self.launch(0)
+
+    def along(self, block, peer):
+        view = self.view(self.rep * self.n + block, None)
+        remote(view, view, self.send_sem, self.line.at[block], (peer, self.rep, self.tp)).start()
 
     def arrive(self, step):
         self.each(step, lambda block: await_heard(self.view(self.rep * self.n + block, None), self.line.at[block]))
+        if self.far and step == self.n - 2:
+            for place, block, peer in ((1, self.n - 1, 0), (self.n - 2, 0, self.n - 1)):
+                pl.when(self.fs == place)(lambda: self.along(block, peer))
         self.launch(step)
 
     def relay(self, step):
@@ -166,21 +175,34 @@
                 todo.append((self.relay, step - 1))
         return todo + ([(self.relay, n - 1)] if n > 1 else [])
 
+    def head(self):
+        return [(self.relay, 0)] + [(self.arrive, step) for step in range(1, self.n - 1)]
+
+    def rest(self):
+        n = self.n
+        return [(self.relay, 1), (self.arrive, n - 1)] + [(self.relay, step) for step in range(2, n)]
+
     def finish(self):
         await_heard(self.many(2 * self.n), self.two_sem)
 
     def drain(self):
-        await_sent(self.many(4 * self.n - 1), self.send_sem)
+        n = self.n
+        for place in range(n):
+            count = 4 * n - 1
+            if self.far:
+                count += -1 if place in (0, n - 1) else 1 if place in (1, n - 2) else 0
+            pl.when(self.fs == place)(lambda: await_sent(self.many(count), self.send_sem))
 
 
 class Scatter:
-    def __init__(self, n, part, one, mid, two, total, out, late, send, one_sem, two_sem, line_sem):
+    def __init__(self, n, direct, part, one, mid, two, total, out, late, send, one_sem, two_sem, line_sem):
         self.n, self.part, self.heard, self.mid_ref, self.two = n, part, one, mid, two
         self.total, self.out, self.late = total, out, late
         self.send_sem, self.one_sem, self.two_sem, self.line_sem = send, one_sem, two_sem, line_sem
         self.fs, self.rep, self.tp = here()
         self.chunks, _, group, self.width = part.shape
         self.rows = group // n
+        self.direct = direct
 
     def peers(self, c):
         first, second = ((1, 2), (2, 1))[c % 2]
@@ -243,6 +265,18 @@
 
     def cross(self, c):
         await_heard(self.two.at[c], self.two_sem.at[c])
+        if c >= self.direct:
+            r = self.rows
+            mine = pl.ds(pl.multiple_of(self.fs * r, r), r)
+            for j in range(1, self.n):
+                f = lax.rem(self.fs + j, self.n)
+                rows = pl.ds(pl.multiple_of(f * r, r), r)
+                self.out[c, rows, :] = self.sums(c, rows).astype(jnp.bfloat16)
+                remote(
+                    self.out.at[c, rows], self.late.at[c, 0, mine], self.send_sem.at[4],
+                    self.line_sem.at[c, 0], (f, self.rep, self.tp),
+                ).start()
+            return
         for place, way in ((0, 0), (self.n - 1, 1)):
             pl.when(self.fs == place)(lambda: self.stream(c, place, way, False))
 
@@ -258,9 +292,16 @@
 
     def final(self, c):
         n, r = self.n, self.rows
+        own = pl.ds(pl.multiple_of(self.fs * r, r), r)
+        if c >= self.direct:
+            value = self.sums(c, own)
+            await_heard(self.late.at[c, 0, pl.ds(0, (n - 1) * r)], self.line_sem.at[c, 0])
+            for j in range(1, n):
+                f = lax.rem(self.fs + j, n)
+                value = value + self.late[c, 0, pl.ds(pl.multiple_of(f * r, r), r), :].astype(jnp.float32)
+            return value
         for place, way in ((0, 1), (n - 1, 0)):
             pl.when(self.fs == place)(lambda: self.hear(c, place, way))
-        own = pl.ds(pl.multiple_of(self.fs * r, r), r)
         self.total[c, own, :] = self.sums(c, own)
         for way, present in ((0, self.fs > 0), (1, self.fs < n - 1)):
 
@@ -274,12 +315,18 @@
         await_sent(self.heard, self.send_sem.at[0])
         await_sent(self.mid_ref, self.send_sem.at[1])
         n, r = self.n, self.rows
+        if self.direct < self.chunks:
+            direct = pl.ds(self.direct, self.chunks - self.direct)
+            await_sent(self.out.at[direct, pl.ds(0, (n - 1) * r)], self.send_sem.at[4])
+        if self.direct == 0:
+            return
         for place in range(n):
 
             def body():
                 for way, count in ((0, n - 1 - place), (1, place)):
                     if count:
-                        await_sent(self.out.at[:, pl.ds(0, count * r)], self.send_sem.at[2 + way])
+                        rows = pl.ds(0, count * r)
+                        await_sent(self.out.at[pl.ds(0, self.direct), rows], self.send_sem.at[2 + way])
 
             pl.when(self.fs == place)(body)
 
@@ -288,15 +335,21 @@
     def __init__(self, n, views, many, send, recv):
         self.lines = [Line(n, v, send.at[i], recv.at[i]) for i, v in enumerate(views)]
         self.n, self.many = n, many
-        self.todo = [(step, line) for step in range(1, n) for line in self.lines]
+        self.todo = [(step, line, None) for step in range(1, n) for line in self.lines]
+
+    def early(self, count):
+        for k in range(count):
+            step, line, _ = self.todo[k]
+            line.start(step, 0)
+            self.todo[k] = (step, line, 1)
 
     def tick(self, count):
         for _ in range(count):
             if self.todo:
-                step, line = self.todo.pop(0)
+                step, line, part = self.todo.pop(0)
                 if step > 1:
                     line.arrive(step - 1)
-                line.start(step)
+                line.start(step, part)
 
     def finish(self):
         self.tick(len(self.todo))
@@ -315,11 +368,11 @@
 def main_kernel(
     n,
     xq_hbm, cq_hbm, xo_hbm, co_hbm, wq_hbm, wo_hbm, bq_hbm, bo_hbm, fq_hbm, sq_hbm, fo_hbm, so_hbm,
-    nq_ref, no_ref, gwq_ref, gwo_ref, hq_ref, ho_ref, nfq_ref, nsq_ref, nfo_ref, nso_ref, tot_ref,
+    uq_ref, uo_ref, gwq_ref, gwo_ref, nfq_ref, nsq_ref, nfo_ref, nso_ref, tot_ref,
     xq, cq, xo, co, wq, wo, fq, sq, fo, so, gbq, gbo, inq, ino,
     part_q, one_q, mid_q, two_q, total_q, out_q, late_q,
     part_o, one_o, mid_o, two_o, total_o, out_o, late_o,
-    gs, local, *sems,
+    nq_ref, no_ref, hq_ref, ho_ref, local, *sems,
 ):
     fs, rep, tp = here()
     mine = rep * n + fs
@@ -364,13 +417,12 @@
 
         return view, lambda k: ref.at[pl.ds(0, k), :, pl.ds(index * 2 * cols, 2 * cols)]
 
-    basis_o = Gather(n, *rows_view(gbo), *take(4))
-    basis_q = Gather(n, *rows_view(gbq), *take(4))
-    norm_o = [Gather(n, *cols_view(no_ref, i, 2), *take(4)) for i in range(2)]
-    norm_q = Gather(n, *cols_view(nq_ref), *take(4))
-    norm_s = Gather(n, *cols_view(gs), *take(4))
-    sum_o = Scatter(n, part_o, one_o, mid_o, two_o, total_o, out_o, late_o, *take(4))
-    sum_q = Scatter(n, part_q, one_q, mid_q, two_q, total_q, out_q, late_q, *take(4))
+    basis_o = Gather(n, False, *rows_view(gbo), *take(4))
+    basis_q = Gather(n, False, *rows_view(gbq), *take(4))
+    norm_o = [Gather(n, True, *cols_view(no_ref, i, 2), *take(4)) for i in range(2)]
+    norm_q = Gather(n, True, *cols_view(nq_ref), *take(4))
+    sum_o = Scatter(n, 3 * part_o.shape[0] // 4, part_o, one_o, mid_o, two_o, total_o, out_o, late_o, *take(4))
+    sum_q = Scatter(n, 0, part_q, one_q, mid_q, two_q, total_q, out_q, late_q, *take(4))
     swap_s, swap_r, share_s, share_r, pair_s, pair_r, weight_s, weight_r = take(8)
 
     views, many = [], []
@@ -387,6 +439,7 @@
     copies[3].wait()
     gwq_ref[fs] = wq[...].astype(b16)
     gwo_ref[fs] = wo[...].astype(b16)
+    weights.early(4)
 
     queue = basis_q.events()
 
@@ -457,17 +510,28 @@
         first_out[:, span] = first_next
         second_out[:, span] = second_next
         n_out[mine, :, span] = normed.astype(b16)
-        square = normed * normed
-        rows, cols = square.shape
-        square = sum(square[:, k : k + 128] for k in range(0, cols, 128))
-        square = sum(square[k : k + 8] for k in range(0, rows, 8))
+
+    def expand(a, first, last):
+        n_ref, h_ref, u_ref = ((nq_ref, hq_ref, uq_ref), (no_ref, ho_ref, uo_ref))[a]
+        rank = n_ref.shape[0] * n_ref.shape[1]
+        wide = 256
         slot = pl.ds(a * 128, 128)
-        gs[mine, :, slot] = square if c == 0 else gs[mine, :, slot] + square
+
+        def step(i, _):
+            span = pl.ds(pl.multiple_of(i * wide, wide), wide)
+            value = n_ref[:, :, span].reshape(rank, wide)
+            u_ref[:, span] = jnp.dot(h_ref[...].reshape(-1, rank), value, preferred_element_type=f32)
+            square = value.astype(f32) * value.astype(f32)
+            square = square[:, :128] + square[:, 128:]
+            tot_ref[0, :, slot] = tot_ref[0, :, slot] + jnp.sum(square.reshape(-1, 8, 128), axis=0)
+            return 0
+
+        lax.fori_loop(first // wide, last // wide, step, 0)
 
     copies[4].wait()
     project(1)
     turn(3)
-    weights.tick(6)
+    weights.tick(10)
     copies[5].wait()
     swapped(1)
     chunks = sum_o.chunks
@@ -481,7 +545,7 @@
             weights.tick(4)
     turn(len(queue))
     keep(1)
-    weights.tick(4)
+    weights.tick(2)
 
     def group(i):
         return range(i * quarter, (i + 1) * quarter)
@@ -490,6 +554,7 @@
         sum_o.middle(c)
     for c in group(2):
         sum_o.send(c)
+    weights.tick(2)
     for c in group(1):
         sum_o.middle(c)
     for c in group(3):
@@ -535,51 +600,51 @@
     weights.tick(1)
     for c in range(sum_q.chunks):
         sum_q.middle(c)
-    onward(3, 0)
     onward(2, 1)
-    weights.tick(1)
     for c in range(sum_q.chunks):
         sum_q.cross(c)
     both(0)
     norm_o[0].start()
-    queue.extend(norm_o[0].events())
-    onward(3, 1)
-    for c in range(sum_q.chunks):
-        sum_q.onward(c, 0)
+    share(1)
+    share(0)
+    keep(0)
     both(2)
     norm_o[1].start()
-    weights.tick(2)
-    for c in range(sum_q.chunks):
-        sum_q.onward(c, 1)
-    turn(2)
-    weights.tick(2)
+    weights.tick(1)
+    queue.extend(norm_o[0].head())
+    turn(len(queue))
     for c in range(sum_q.chunks):
         norm(0, c, sum_q)
     norm_q.start()
-    norm_s.start()
-    weights.tick(4)
-    turn(1)
-    share(1)
-    share(0)
-    keep(0)
+    tot_ref[0] = jnp.zeros(tot_ref.shape[1:], f32)
+    queue.extend(norm_o[1].head())
     turn(len(queue))
-    later = [*zip(norm_o[1].events(), norm_q.events(), norm_s.events())]
-    for k, steps in enumerate(later):
-        for action, step in steps:
-            action(step)
+    queue.extend(norm_q.head())
+    turn(len(queue))
+    weights.tick(2)
+    columns = no_ref.shape[2]
+    first, second, last = norm_o[0].rest(), norm_o[1].rest(), norm_q.rest()
+    for k in range(n + 2):
+        for steps, lag in ((first, 0), (second, 1), (last, 2)):
+            queue.extend(steps[k - lag : k - lag + 1] if k >= lag else [])
+        turn(len(queue))
         weights.tick(2)
-    norms = (*norm_o, norm_q, norm_s)
-    for g in norms:
-        g.finish()
-    tot_ref[0] = sum(gs[b] for b in range(4 * n))
+        if k == n:
+            shared(1)
+            norm_o[0].finish()
+            expand(1, 0, columns // 2)
+    norm_o[1].finish()
+    expand(1, columns // 2, columns)
+    shared(0)
+    norm_q.finish()
+    expand(0, 0, nq_ref.shape[2])
     pair = remote(tot_ref.at[0], tot_ref.at[1], pair_s.at[0], pair_r.at[0], (fs, rep, 1 - tp))
     pair.start()
     weights.finish()
     pair.wait()
     for a in (0, 1):
         await_sent((inq, ino)[a].at[tp], swap_s.at[a])
-        shared(a)
-    for g in (basis_o, basis_q, *norms, sum_o, sum_q):
+    for g in (basis_o, basis_q, *norm_o, norm_q, sum_o, sum_q):
         g.drain()
     weights.sent()
 
@@ -606,29 +671,29 @@
 
     pieces = sum(pieces_of(wq, wo))
     gather = [(), (n,), (2, n), ()]
-    reduce = lambda chunks: [(4,), (chunks,), (chunks,), (chunks, 2)]
-    shapes = gather * 6 + reduce(8) + reduce(2) + [(2,), (2,), (2,), (2,), (1,), (1,), (pieces, 2), (pieces, n)]
+    reduce = lambda chunks: [(5,), (chunks,), (chunks,), (chunks, 2)]
+    shapes = gather * 5 + reduce(8) + reduce(2) + [(2,), (2,), (2,), (2,), (1,), (1,), (pieces, 2), (pieces, n)]
     spec = pl.BlockSpec(memory_space=pltpu.VMEM)
     return pl.pallas_call(
         functools.partial(main_kernel, n),
         out_shape=(
-            shape((4 * n, rows, cq.shape[1]), b16),
-            shape((4 * n, rows, co.shape[1]), b16),
+            shape((n * bq.shape[0], cq.shape[1]), f32),
+            shape((n * bo.shape[0], co.shape[1]), f32),
             shape((n, *wq.shape), b16),
             shape((n, *wo.shape), b16),
-            shape((n, *bq.shape), b16),
-            shape((n, *bo.shape), b16),
             *[shape(a.shape, f32) for a in (fq, sq, fo, so)],
             shape((2, 8, 256), f32),
         ),
         in_specs=[pl.BlockSpec(memory_space=pltpu.HBM)] * 12,
-        out_specs=(spec,) * 11,
+        out_specs=(spec,) * 9,
         scratch_shapes=[vmem(a.shape, a.dtype) for a in (xq, cq, xo, co, wq, wo, fq, sq, fo, so)]
         + [vmem((4 * n, bq.shape[0], half), b16), vmem((4 * n, bo.shape[0], half), b16)]
         + [vmem((2, half, xq.shape[0]), b16), vmem((2, half, xo.shape[0]), b16)]
         + scatter(2, width_q)
         + scatter(8, width_o)
-        + [vmem((4 * n, 8, 256), f32), DMA((12,))]
+        + [vmem((4 * n, rows, a.shape[1]), b16) for a in (cq, co)]
+        + [vmem((n, *a.shape), b16) for a in (bq, bo)]
+        + [DMA((12,))]
         + [DMA(a) if a else DMA for a in shapes],
         compiler_params=pltpu.CompilerParams(
             collective_id=0, has_side_effects=True, vmem_limit_bytes=40 * 2**20
@@ -639,12 +704,13 @@
 
 def last_kernel(
     n,
-    hq, ho, nq, no, gwq, gwo, nfq, nsq, nfo, nso, tot,
+    uq, uo, gwq, gwo, nfq, nsq, nfo, nso, tot,
     uq_out, uo_out, nfq_out, nsq_out, nfo_out, nso_out, cq_out, co_out,
-    uq, uo, cq, co, sems,
+    mq, mo, cq, co, sems,
 ):
     fs = lax.axis_index("fs")
     f32, b16 = jnp.float32, jnp.bfloat16
+    rank = 4 * n * nfq.shape[0]
     copies = []
 
     def put(src, dst):
@@ -654,31 +720,30 @@
 
     for src, dst in ((nfq, nfq_out), (nsq, nsq_out), (nfo, nfo_out), (nso, nso_out)):
         put(src, dst)
-    rank = nq.shape[0]
-    for a, (rows_ref, normed, weights, u, c, u_hbm, c_hbm) in enumerate(
-        ((hq, nq, gwq, uq, cq, uq_out, cq_out), (ho, no, gwo, uo, co, uo_out, co_out))
+    for a, (u, weights, m, c, m_hbm, c_hbm) in enumerate(
+        ((uq, gwq, mq, cq, uq_out, cq_out), (uo, gwo, mo, co, uo_out, co_out))
     ):
-        columns = normed.shape[1]
+        rows, columns = u.shape
         total = jnp.sum(tot[:, :, a * 128 : (a + 1) * 128], axis=0)
         total = jnp.sum(jnp.sum(total, axis=0, keepdims=True), axis=1, keepdims=True)
         scale = lax.rsqrt(total / (rank * 2 * columns) + small_eps)
-        tile = min(256, columns)
-        mine = u_hbm.shape[0]
-        block = 2 * tile if columns % (2 * tile) == 0 else tile
-
-        for k in range(0, columns, block):
+        mine = m.shape[0]
+        own = pl.ds(pl.multiple_of(fs * mine, mine), mine)
+        m[...] = scale * u[own, :]
+        put(m, m_hbm)
+        block = min(128, rows)
+
+        for k in range(0, rows, block):
 
             def step(i, _):
-                span = pl.ds(pl.multiple_of(k + i * tile, tile), tile)
-                value = scale * jnp.dot(rows_ref[...], normed[:, span], preferred_element_type=f32)
-                u[:, span] = value
-                c[:, span] = (weights[:, span].astype(f32) - step_rate * value).astype(b16)
+                span = pl.ds(pl.multiple_of(k + i * 16, 16), 16)
+                value = scale * u[span, :]
+                c[span, :] = (weights[span, :].astype(f32) - step_rate * value).astype(b16)
                 return 0
 
-            lax.fori_loop(0, block // tile, step, 0)
+            lax.fori_loop(0, block // 16, step, 0)
             span = pl.ds(k, block)
-            put(u.at[pl.ds(pl.multiple_of(fs * mine, mine), mine), span], u_hbm.at[:, span])
-            put(c.at[:, span], c_hbm.at[:, span])
+            put(c.at[span], c_hbm.at[span])
     for copy in copies:
         copy.wait()
 
@@ -686,27 +751,25 @@
 def body(n, *args):
     xq, cq, xo, co, wq, wo, bq, bo, fq, sq, fo, so = args
     f32, b16 = jnp.float32, jnp.bfloat16
-    rank = bq.shape[1]
-    nq, no, gwq, gwo, hq, ho, nfq, nsq, nfo, nso, tot = advance(n, *args)
+    uq, uo, gwq, gwo, nfq, nsq, nfo, nso, tot = advance(n, *args)
     shape, vmem = jax.ShapeDtypeStruct, pltpu.VMEM
-    flat = lambda a: a.reshape(-1, a.shape[2])
-    hq, ho, nq, no, gwq, gwo = [flat(a) for a in (hq, ho, nq, no, gwq, gwo)]
+    gwq, gwo = [a.reshape(-1, a.shape[2]) for a in (gwq, gwo)]
     outs = (
         shape(wq.shape, f32), shape(wo.shape, f32), shape(fq.shape, f32), shape(fq.shape, f32),
         shape(fo.shape, f32), shape(fo.shape, f32), shape(gwq.shape, b16), shape(gwo.shape, b16),
     )
-    wide = lambda a: vmem(a.shape, f32)
     spec = pl.BlockSpec(memory_space=pltpu.VMEM)
     return pl.pallas_call(
         functools.partial(last_kernel, n),
         out_shape=outs,
-        in_specs=[spec] * 11,
+        in_specs=[spec] * 9,
         out_specs=(pl.BlockSpec(memory_space=pl.ANY),) * 8,
-        scratch_shapes=[wide(gwq), wide(gwo)]
-        + [vmem(gwq.shape, b16), vmem(gwo.shape, b16), DMA((4 + 2 + 2 * (wo.shape[1] // 256),))],
+        scratch_shapes=[vmem(wq.shape, f32), vmem(wo.shape, f32)]
+        + [vmem(gwq.shape, b16), vmem(gwo.shape, b16)]
+        + [DMA((6 + sum(-(-a.shape[0] // 128) for a in (gwq, gwo)),))],
         compiler_params=pltpu.CompilerParams(vmem_limit_bytes=20 * 2**20),
         name="update",
-    )(hq, ho, nq, no, gwq, gwo, nfq, nsq, nfo, nso, tot)
+    )(uq, uo, gwq, gwo, nfq, nsq, nfo, nso, tot)
 
 
 def solution(mesh):

time: 105 us -> 101 us (0.962)
  Pallas kernels: 104 us -> 100 us
    pallas_call x1, Pallas kernels: 99.8 us -> 97.4 us  [advance(): pl.pallas_call(functools.partial(main_kernel, n), out_shape=(shape((n * b...]
    pallas_call x1, Pallas kernels: 4.63 us -> 2.82 us  [body(): pl.pallas_call(functools.partial(last_kernel, n), out_shape=outs, in_spec...]
where the time goes in v4:
time: 101 us
  Pallas kernels  100 us (99%)
    pallas_call x1, Pallas kernels, advance(): pl.pallas_call(functools.partial(main_kernel, n), out_shape=(shape((n * b...  97.4 us
    pallas_call x1, Pallas kernels, body(): pl.pallas_call(functools.partial(last_kernel, n), out_shape=outs, in_spec...  2.82 us

profile of v4, /device:TPU:0, one launch (start us, length us, event | category | flops | bytes accessed | tf_op | source)
XLA Modules:
  0.0 100.9 jit_solution(16908520007535217692)
XLA Ops:
  0.6 97.4 %advance.1 = (f32[1024,512]{1,0:T(8,128)S(1)}, f32[512,2048]{1,0:T(8,128)S(1)}, bf16[4,256,512]{2,1,0:T(8,128)(2,1)S(1)}, bf16[4,128,2048]{2,1,0:T(8,128)(2,1)S(...) custom-call(bf16[1024,4096]{1,0:T(8,128)(2,1)} %xq_hbm.1, ...), custom_call_target="tpu_custom_call" | custom-call | tf_op jit(solution)/shard_map/advance/pallas_call | solution.py:677
  98.0 2.8 %update.1 = (f32[256,512]{1,0:T(8,128)}, f32[128,2048]{1,0:T(8,128)}, f32[32,512]{1,0:T(8,128)}, f32[32,512]{1,0:T(8,128)}, f32[32,2048]{1,0:T(8,128)}, /*index=...) custom-call(f32[1024,512]{1,0:T(8,128)S(1)} %get-tuple-element.17.uq, ...), custom_call_target="tpu_custom_call" | custom-call | tf_op jit(solution)/shard_map/update/pallas_call | solution.py:762

commit v5 on v4

--- a/solution.py
+++ b/solution.py
@@ -333,7 +333,8 @@
 
 class Weights:
     def __init__(self, n, views, many, send, recv):
-        self.lines = [Line(n, v, send.at[i], recv.at[i]) for i, v in enumerate(views)]
+        self.lines = [Line(n, view, send.at[a], recv.at[i]) for i, (a, view) in enumerate(views)]
+        self.last = [Line(n, None, send.at[a], None) for a in range(len(many))]
         self.n, self.many = n, many
         self.todo = [(step, line, None) for step in range(1, n) for line in self.lines]
 
@@ -357,7 +358,7 @@
             line.arrive(self.n - 1)
 
     def sent(self):
-        for line, many in zip(self.lines, self.many):
+        for line, many in zip(self.last, self.many):
             line.sent(many)
 
 
@@ -426,11 +427,11 @@
     swap_s, swap_r, share_s, share_r, pair_s, pair_r, weight_s, weight_r = take(8)
 
     views, many = [], []
-    for ref, pieces in zip((gwq_ref, gwo_ref), pieces_of(gwq_ref, gwo_ref)):
+    for a, (ref, pieces) in enumerate(zip((gwq_ref, gwo_ref), pieces_of(gwq_ref, gwo_ref))):
         rows = ref.shape[1] // pieces
+        many.append(lambda k, ref=ref: ref.at[pl.ds(0, k)])
         for p in range(pieces):
-            views.append(lambda b, ref=ref, p=p, rows=rows: ref.at[b, pl.ds(p * rows, rows)])
-            many.append(lambda k, ref=ref, p=p, rows=rows: ref.at[pl.ds(0, k), pl.ds(p * rows, rows)])
+            views.append((a, lambda b, ref=ref, p=p, rows=rows: ref.at[b, pl.ds(p * rows, rows)]))
     weights = Weights(n, views, many, weight_s, weight_r)
 
     basis_o.start()
@@ -610,7 +611,7 @@
     keep(0)
     both(2)
     norm_o[1].start()
-    weights.tick(1)
+    weights.tick(2)
     queue.extend(norm_o[0].head())
     turn(len(queue))
     for c in range(sum_q.chunks):
@@ -672,7 +673,7 @@
     pieces = sum(pieces_of(wq, wo))
     gather = [(), (n,), (2, n), ()]
     reduce = lambda chunks: [(5,), (chunks,), (chunks,), (chunks, 2)]
-    shapes = gather * 5 + reduce(8) + reduce(2) + [(2,), (2,), (2,), (2,), (1,), (1,), (pieces, 2), (pieces, n)]
+    shapes = gather * 5 + reduce(8) + reduce(2) + [(2,), (2,), (2,), (2,), (1,), (1,), (2, 2), (pieces, n)]
     spec = pl.BlockSpec(memory_space=pltpu.VMEM)
     return pl.pallas_call(
         functools.partial(main_kernel, n),

time: 101 us -> 100 us (0.990)
  no operation moved by 1% of the time
where the time goes in v5:
time: 100 us; the launch traced here: 99.9 us
  Pallas kernels  99.3 us (99%)
    pallas_call x1, Pallas kernels, advance(): pl.pallas_call(functools.partial(main_kernel, n), out_shape=(shape((n * b...  96.4 us
    pallas_call x1, Pallas kernels, body(): pl.pallas_call(functools.partial(last_kernel, n), out_shape=outs, in_spec...  2.82 us

profile of v5, /device:TPU:0, one launch (start us, length us, event | category | flops | bytes accessed | tf_op | source)
XLA Modules:
  0.0 99.9 jit_solution(16737871125767083674)
XLA Ops:
  0.6 96.4 %advance.1 = (f32[1024,512]{1,0:T(8,128)S(1)}, f32[512,2048]{1,0:T(8,128)S(1)}, bf16[4,256,512]{2,1,0:T(8,128)(2,1)S(1)}, bf16[4,128,2048]{2,1,0:T(8,128)(2,1)S(...) custom-call(bf16[1024,4096]{1,0:T(8,128)(2,1)} %xq_hbm.1, ...), custom_call_target="tpu_custom_call" | custom-call | tf_op jit(solution)/shard_map/advance/pallas_call | solution.py:678
  97.1 2.8 %update.1 = (f32[256,512]{1,0:T(8,128)}, f32[128,2048]{1,0:T(8,128)}, f32[32,512]{1,0:T(8,128)}, f32[32,512]{1,0:T(8,128)}, f32[32,2048]{1,0:T(8,128)}, /*index=...) custom-call(f32[1024,512]{1,0:T(8,128)S(1)} %get-tuple-element.17.uq, ...), custom_call_target="tpu_custom_call" | custom-call | tf_op jit(solution)/shard_map/update/pallas_call | solution.py:763
